TPU v7x, 32 devices: a whole 2x2x4 slice. The times are simulated.
32 devices in a mesh: sp: 8 (over z, y), tp: 4 (over x, core).
Axes of the slice: x: 2, y: 2, z: 4, core: 2. Of those that a mesh axis runs over, the one named last changes fastest.
Arguments:
- grouped_head_inputs: bfloat16 [8192, 2, 1024], P('sp', None, 'tp'), may hold values from -6 to 6
- head_gate_inputs: bfloat16 [8192, 2, 1024], P('sp', None, 'tp'), may hold values from -6 to 6
- unsmoothed_step: float32 [8192, 2, 16], P('sp', None, 'tp'), may hold values from -3.8 to 3.8
- head_decay_rate: float32 [2, 16], P(None, 'tp'), may hold values from 1.2207031e-05 to 0.04761905
- extra_log_decay: float32 [8192, 2, 16], P('sp', None, 'tp'), may hold values from -1.4 to 0
- first_group_keys: bfloat16 [8192, 128], P('sp'), may hold values from -6 to 6
- first_group_queries: bfloat16 [8192, 128], P('sp'), may hold values from -6 to 6
- second_group_keys: bfloat16 [8192, 64], P('sp'), may hold values from -6 to 6
- second_group_queries: bfloat16 [8192, 64], P('sp'), may hold values from -6 to 6
- head_input_filter: float32 [4, 2, 1024], P(None, None, 'tp'), may hold values from -3 to 3
- first_group_filter: float32 [4, 2, 128], replicated, may hold values from -3 to 3
- second_group_filter: float32 [4, 2, 64], replicated, may hold values from -3 to 3
- head_norm_gain: float32 [2, 1024], P(None, 'tp'), may hold values from 0.1 to 1.9
- output_weight: bfloat16 [2, 1024, 2048], P(None, None, 'tp'), may hold values from -0.125 to 0.125
- residual: bfloat16 [8192, 2048], P('sp', 'tp'), may hold values from -37 to 37
- channel_norm_gain: float32 [2048], replicated, may hold values from 0.1 to 1.9
- channel_gate_weight: bfloat16 [2048, 5120], P('sp', 'tp'), may hold values from -0.125 to 0.125
- channel_up_weight: bfloat16 [2048, 5120], P('sp', 'tp'), may hold values from -0.125 to 0.125
- channel_down_weight: bfloat16 [2048, 5120], P('sp', 'tp'), may hold values from -0.078125 to 0.078125
Outputs:
- layer_output: bfloat16 [8192, 2048], P('sp', 'tp')
All inputs are finite; a program needn't handle non-finite values.
Results may differ from a plain program's by a relative error of at most 0.007.
Values may be sent and summed in bfloat16 or wider, within the bound.
A program may use at most 128 MiB of HBM per device.

v0:
```python
import functools

import jax
import jax.numpy as jnp
from jax import lax
from jax.experimental import pallas as pl
from jax.experimental.pallas import tpu as pltpu
from jax.sharding import PartitionSpec as P

HEAD = 64
CONV = 4
BLOCK = 128
RIM = 16
EPSILON = 1e-06
LANES = 128
VMEM_LIMIT = 63 << 20
MESH = pl.DeviceIdType.MESH


def rows_of(b):
    return pl.ds(pl.multiple_of(b * BLOCK, BLOCK), BLOCK)


def spread(columns, first, count):
    parts = [
        jnp.broadcast_to(columns[:, h : h + 1], (columns.shape[0], HEAD))
        for h in range(first, first + count)
    ]
    return jnp.concatenate(parts, axis=1)


def sigmoid(x):
    return 1.0 / (1.0 + jnp.exp(-x))


def layer_kernel(
    n, tp, heads, s1, s2, split,
    x_ref, gate_ref, log_ref, step_ref, taps_ref, hgain_ref, wout_ref, res_ref, cgain_ref,
    wg_ref, wu_ref, wd_ref,
    out_ref,
    xs, rim, vals, kq, cums, st, stsend, strecv, mix, stream, normed, weights, hidden,
    give, give_recv, sums, sums_recv,
    rim_sems, st_send, st_recv, m_send, m_fwd, m_recv, r_send, r_fwd, r_recv,
    p_send, p_fwd, p_recv, w_local, w_pair, w_send, w_recv, g_send, g_recv, s_send, s_recv,
):
    me = lax.axis_index("sp")
    t = lax.axis_index("tp")
    half = heads * HEAD
    wide = 2 * half
    nb = x_ref.shape[0] // BLOCK
    nx = tp // 2
    core = lax.rem(t, 2)
    my_x = t // 2
    partner = my_x * 2 + (1 - core)

    m = n // 2
    q = me // 2
    y = lax.rem(me, 2)
    pair = q * 2 + (1 - y)
    shard = wg_ref.shape[-2]
    tokens = x_ref.shape[0]
    sources = (wg_ref, wu_ref, wd_ref)
    part = weights.shape[2]

    def half_of(w, which):
        if split:
            return sources[w].at[which]
        return sources[w].at[:, pl.ds(pl.multiple_of(which * part, part), part)]

    def unit(w, s):
        return weights.at[w, pl.ds(pl.multiple_of(s * shard, shard), shard)]

    def keep_own(w):
        return pltpu.make_async_copy(half_of(w, y), unit(w, me), w_local.at[w])

    def give_pair(w):
        return pltpu.make_async_remote_copy(
            src_ref=half_of(w, 1 - y),
            dst_ref=unit(w, me),
            send_sem=w_pair.at[w],
            recv_sem=w_recv.at[w, me],
            device_id={"sp": pair},
            device_id_type=MESH,
        )

    def along(w, s, up, own=False):
        return pltpu.make_async_remote_copy(
            src_ref=half_of(w, y) if own else unit(w, s),
            dst_ref=unit(w, s),
            send_sem=w_send.at[int(up), w, s],
            recv_sem=w_recv.at[w, s],
            device_id={"sp": lax.rem(me + 2, n) if up else lax.rem(me + n - 2, n)},
            device_id_type=MESH,
        )

    def send_along(w, s, up, own=False):
        @pl.when(q < m - 1 if up else q > 0)
        def _():
            along(w, s, up, own).start()

    def take_unit(w, s):
        along(w, s, True).wait_recv()

    def start_weights():
        for w in range(2):
            give_pair(w).start()
            send_along(w, me, False, own=True)
            send_along(w, me, True, own=True)
        give_pair(2).start()
        for w in range(3):
            keep_own(w).start()

    def relay(w, d, sel):
        other = lax.rem(y + sel, 2)

        @pl.when(q + d < m)
        def _():
            s = (q + d) * 2 + other
            take_unit(w, s)
            send_along(w, s, False)

            @pl.when(d == 0)
            def _():
                send_along(w, s, True)

        @pl.when((d > 0) & (q - d >= 0))
        def _():
            s = (q - d) * 2 + other
            take_unit(w, s)
            send_along(w, s, True)

    def relay_step(k):
        relay(lax.rem(k, 2), k // 4, lax.rem(k // 2, 2))

    early = 4 * (m - 1)
    points = nb // 2 + (nb + 4) // 2
    per_point = pl.cdiv(max(early - 2, 0), points)

    def relay_point(p):
        for i in range(per_point):
            k = 2 + p * per_point + i

            @pl.when(k < early)
            def _():
                relay_step(k)

    rim_copy = pltpu.make_async_remote_copy(
        src_ref=x_ref.at[pl.ds(x_ref.shape[0] - RIM, RIM)],
        dst_ref=rim,
        send_sem=rim_sems.at[0],
        recv_sem=rim_sems.at[1],
        device_id={"sp": lax.rem(me + 1, n)},
        device_id_type=MESH,
    )

    @pl.when(me < n - 1)
    def _():
        rim_copy.start()

    start_weights()

    @pl.when(me > 0)
    def _():
        rim_copy.wait_recv()
        xs[...] = rim[...].astype(jnp.float32)[RIM - 8 :]

    @pl.when(me == 0)
    def _():
        xs[...] = jnp.zeros_like(xs)

    st[...] = jnp.zeros_like(st)
    row_i = lax.broadcasted_iota(jnp.int32, (BLOCK, BLOCK), 0)
    col_i = lax.broadcasted_iota(jnp.int32, (BLOCK, BLOCK), 1)
    causal = row_i >= col_i
    tri = jnp.where(causal, 1.0, 0.0).astype(jnp.float32)

    def state_update(b, cum):
        last = cum[BLOCK - 1 : BLOCK]
        to_end = jnp.exp(last - cum)
        decay = jnp.exp(last)
        r = rows_of(b)
        for g in range(2):
            k0, size = (wide, s1) if g == 0 else (wide + 2 * s1, s2)
            base = 0 if g == 0 else s1
            keys = kq[r, k0 - wide : k0 - wide + size]
            v = vals[r, g * half : (g + 1) * half].astype(jnp.float32)
            v = (v * spread(to_end, g * heads, heads)).astype(jnp.bfloat16)
            add = lax.dot_general(
                keys, v, (((0,), (0,)), ((), ())), preferred_element_type=jnp.float32
            )
            st[base : base + size] = (
                st[base : base + size] * spread(decay, g * heads, heads) + add
            )

    def first_pass(b, total):
        r = rows_of(b)
        current = x_ref[r].astype(jnp.float32)
        taps = taps_ref[...]
        extended = jnp.concatenate([xs[...], current], axis=0)
        acc = taps[CONV - 1 : CONV] * current
        for k in range(CONV - 1):
            acc = acc + taps[k : k + 1] * pltpu.roll(extended, CONV - 1 - k, 0)[8:]
        xs[...] = current[BLOCK - 8 :]
        acc = acc * sigmoid(acc)
        vals[r] = (acc[:, :wide] * spread(step_ref[r], 0, 2 * heads)).astype(jnp.bfloat16)
        kq[r] = acc[:, wide:].astype(jnp.bfloat16)
        cum = jnp.dot(
            tri, log_ref[r], precision=lax.Precision.HIGHEST, preferred_element_type=jnp.float32
        )
        cums[r] = cum
        state_update(b, cum)

        @pl.when(lax.rem(b, 2) == 1)
        def _():
            relay_point(b // 2)

        return total + cum[BLOCK - 1 : BLOCK]

    total = lax.fori_loop(0, nb, first_pass, jnp.zeros((1, log_ref.shape[1]), jnp.float32))

    states = s1 + s2
    stsend[0:states] = st[...].astype(jnp.bfloat16)
    which = lax.broadcasted_iota(jnp.int32, (RIM, half), 0)
    extra = jnp.zeros((RIM, half), jnp.float32)
    for g in range(2):
        logs = spread(total, g * heads, heads)
        high = logs.astype(jnp.bfloat16).astype(jnp.float32)
        low = logs - high
        extra = jnp.where(which == g, high, extra)
        extra = jnp.where(which == 2 + g, low, extra)
    stsend[states : states + RIM] = extra.astype(jnp.bfloat16)

    def state_copy(to, source):
        return pltpu.make_async_remote_copy(
            src_ref=stsend,
            dst_ref=strecv.at[source],
            send_sem=st_send.at[to],
            recv_sem=st_recv.at[source],
            device_id={"sp": to},
            device_id_type=MESH,
        )

    def send_state(to, carry):
        state_copy(to, me).start()
        return carry

    lax.fori_loop(me + 1, n, send_state, 0)
    st[...] = jnp.zeros_like(st)

    def take_state(source, carry):
        state_copy(n - 1, source).wait_recv()
        got = strecv[source].astype(jnp.float32)
        for g in range(2):
            base, size = (0, s1) if g == 0 else (s1, s2)
            logs = got[states + g : states + g + 1] + got[states + 2 + g : states + 3 + g]
            st[base : base + size] = st[base : base + size] * jnp.exp(logs) + got[base : base + size]
        return carry

    lax.fori_loop(0, me, take_state, 0)

    def share(buf, yy, source, b, sp, to, send, recv):
        piece = buf.at[yy, source, rows_of(b)]
        return pltpu.make_async_remote_copy(
            src_ref=piece,
            dst_ref=piece,
            send_sem=send,
            recv_sem=recv.at[source, b],
            device_id={"sp": sp, "tp": to},
            device_id_type=MESH,
        )

    def across(d):
        return lax.rem(my_x + d, nx) * 2

    def send_own(buf, yy, b, send, recv):
        for d in range(1, nx):
            to = across(d) + core
            share(buf, yy, t, b, me, to, send.at[d, b], recv).start()
        share(buf, yy, t, b, me, partner, send.at[0, b], recv).start()

    def forward(buf, yy, b, fwd, recv):
        for d in range(1, nx):
            source = across(d) + core
            move = share(buf, yy, source, b, me, partner, fwd.at[d, b], recv)
            move.wait_recv()
            move.start()

    def wait_rest(buf, yy, b, send, recv):
        share(buf, yy, partner, b, me, partner, send.at[0, b], recv).wait_recv()
        for d in range(1, nx):
            source = across(d) + (1 - core)
            share(buf, yy, source, b, me, partner, send.at[0, b], recv).wait_recv()

    def send_pair(b):
        for d in range(nx):
            to = across(d) + core
            share(stream, y, t, b, pair, to, p_send.at[d, b], p_recv).start()

    def forward_pair(b):
        for d in range(nx):
            source = across(d) + core
            move = share(stream, 1 - y, source, b, me, partner, p_fwd.at[d, b], p_recv)
            move.wait_recv()
            move.start()

    def wait_pair(b):
        for d in range(nx):
            source = across(d) + (1 - core)
            share(stream, 1 - y, source, b, me, partner, p_fwd.at[d, b], p_recv).wait_recv()

    def second_pass(b):
        r = rows_of(b)
        cum = cums[r]
        cum_t = cum.T
        grown = jnp.exp(cum)
        for g in range(2):
            off, size = (0, s1) if g == 0 else (2 * s1, s2)
            base = 0 if g == 0 else s1
            keys = kq[r, off : off + size]
            queries = kq[r, off + size : off + 2 * size]
            scores = lax.dot_general(
                queries, keys, (((1,), (1,)), ((), ())), preferred_element_type=jnp.float32
            )
            carried = jnp.dot(
                queries,
                st[base : base + size].astype(jnp.bfloat16),
                preferred_element_type=jnp.float32,
            )
            carried = carried * spread(grown, g * heads, heads)
            v = vals[r, g * half : (g + 1) * half]
            outs = []
            for h in range(heads):
                c = g * heads + h
                span = jnp.where(causal, cum[:, c : c + 1] - cum_t[c : c + 1, :], -jnp.inf)
                w = (jnp.exp(span) * scores).astype(jnp.bfloat16)
                lanes = slice(h * HEAD, (h + 1) * HEAD)
                y = jnp.dot(w, v[:, lanes], preferred_element_type=jnp.float32)
                y = y + carried[:, lanes]
                z = gate_ref[r, g * half + h * HEAD : g * half + (h + 1) * HEAD].astype(jnp.float32)
                y = y * (z * sigmoid(z))
                y = y * lax.rsqrt(jnp.mean(y * y, axis=1, keepdims=True) + EPSILON)
                outs.append(y)
            out = jnp.concatenate(outs, axis=1) * hgain_ref[:, g * half : (g + 1) * half]
            mix[0, t, r, g * half : (g + 1) * half] = out.astype(jnp.bfloat16)
        state_update(b, cum)
        send_own(mix, 0, b, m_send, m_recv)

    def project(b):
        r = rows_of(b)
        wait_rest(mix, 0, b, m_send, m_recv)
        acc = res_ref[r].astype(jnp.float32)
        for source in range(tp):
            acc = acc + jnp.dot(
                mix[0, source, r], wout_ref[source], preferred_element_type=jnp.float32
            )
        stream[y, t, r] = acc.astype(jnp.bfloat16)
        send_own(stream, y, b, r_send, r_recv)
        send_pair(b)

    cols = res_ref.shape[1]

    def normalise(yy, b):
        r = rows_of(b)
        parts = [stream[yy, source, r].astype(jnp.float32) for source in range(tp)]
        square = sum(jnp.sum(p * p, axis=1, keepdims=True) for p in parts)
        scale = lax.rsqrt(square / (tp * cols) + EPSILON)
        for source in range(tp):
            lanes = slice(source * cols, (source + 1) * cols)
            normed[yy, r, lanes] = (parts[source] * scale * cgain_ref[:, lanes]).astype(
                jnp.bfloat16
            )

    def stage(b, carry):
        @pl.when(b < nb)
        def _():
            second_pass(b)

        @pl.when(lax.rem(b, 2) == 0)
        def _():
            relay_point(nb // 2 + b // 2)

        @pl.when((b >= 1) & (b < nb + 1))
        def _():
            forward(mix, 0, b - 1, m_fwd, m_recv)

        @pl.when((b >= 2) & (b < nb + 2))
        def _():
            project(b - 2)

        @pl.when((b >= 3) & (b < nb + 3))
        def _():
            forward(stream, y, b - 3, r_fwd, r_recv)
            forward_pair(b - 3)

        @pl.when(b >= 4)
        def _():
            wait_rest(stream, y, b - 4, r_send, r_recv)
            normalise(y, b - 4)
            wait_pair(b - 4)
            normalise(1 - y, b - 4)

        return carry

    lax.fori_loop(0, nb + 4, stage, 0)

    down = 2
    send_along(down, me, False, own=True)
    send_along(down, me, True, own=True)
    take_unit(down, pair)
    send_along(down, pair, False)
    send_along(down, pair, True)

    def late(k, carry):
        relay_step(k)
        return carry

    lax.fori_loop(early, 4 * m, late, 0)
    for w in range(3):
        keep_own(w).wait()

    tall = 2 * BLOCK
    pieces = tokens // tall

    def mix_channels(i, carry):
        yy = i // pieces
        r = pl.ds(pl.multiple_of(lax.rem(i, pieces) * tall, tall), tall)
        rows = normed[yy, r]
        g = jnp.dot(rows, weights[0], preferred_element_type=jnp.float32)
        u = jnp.dot(rows, weights[1], preferred_element_type=jnp.float32)
        hidden[yy, r] = (g * sigmoid(g) * u).astype(jnp.bfloat16)
        return carry

    lax.fori_loop(0, 2 * pieces, mix_channels, 0)

    near = jnp.minimum(q, m - 1 - q)

    def block_at(i):
        d = (i + 1) // 2
        side = jnp.where(lax.rem(i, 2) == 1, q + d, q - d)
        beyond = jnp.where(q < m - 1 - q, i, m - 1 - i)
        return jnp.where(i <= 2 * near, side, beyond)

    width = sums.shape[2]
    units = width // shard
    chunks = tp * cols // width
    per_owner = cols // width

    def shard_at(i):
        return block_at(i // 2) * 2 + lax.rem(y + lax.rem(i, 2), 2)

    def take_down(i):
        s = shard_at(i)

        @pl.when(i >= 2)
        def _():
            take_unit(down, s)

            @pl.when(s > me)
            def _():
                send_along(down, s, False)

            @pl.when(s < me)
            def _():
                send_along(down, s, True)

    def chunk_at(i):
        return shard_at(i) if units == 1 else i

    def product(yy, k, p):
        r = pl.ds(pl.multiple_of(p * tall, tall), tall)
        block = weights[down, pl.ds(pl.multiple_of(k * width, width), width)]
        return lax.dot_general(
            hidden[yy, r], block, (((1,), (1,)), ((), ())), preferred_element_type=jnp.float32
        )

    def give_copy(i, k):
        return pltpu.make_async_remote_copy(
            src_ref=give.at[lax.rem(i, 2)],
            dst_ref=give_recv.at[k],
            send_sem=g_send.at[lax.rem(i, 2)],
            recv_sem=g_recv.at[k],
            device_id={"tp": partner},
            device_id_type=MESH,
        )

    mine = my_x * 2 + y

    def sum_copy(i, k, source):
        return pltpu.make_async_remote_copy(
            src_ref=sums.at[lax.rem(i, 2)],
            dst_ref=sums_recv.at[source, lax.rem(k, per_owner)],
            send_sem=s_send.at[lax.rem(i, 2)],
            recv_sem=s_recv.at[source, lax.rem(k, per_owner)],
            device_id={"sp": q * 2 + core, "tp": k // per_owner},
            device_id_type=MESH,
        )

    def to_self(k):
        return (k // per_owner == t) & (y == core)

    def give_half(i):
        k = chunk_at(i)

        @pl.when(i >= 2)
        def _():
            give_copy(i, k).wait_send()

        def one(p, carry):
            r = pl.ds(pl.multiple_of(p * tall, tall), tall)
            give[lax.rem(i, 2), r] = product(1 - core, k, p).astype(jnp.bfloat16)
            return carry

        lax.fori_loop(0, pieces, one, 0)
        give_copy(i, k).start()

    def sum_half(i):
        k = chunk_at(i)

        @pl.when(i >= 2)
        def _():
            before = chunk_at(i - 2)

            @pl.when(jnp.logical_not(to_self(before)))
            def _():
                sum_copy(i, before, mine).wait_send()

        give_copy(i, k).wait_recv()

        def one(p, carry):
            r = pl.ds(pl.multiple_of(p * tall, tall), tall)
            both = product(core, k, p) + give_recv[k, r].astype(jnp.float32)
            sums[lax.rem(i, 2), r] = both.astype(jnp.bfloat16)
            return carry

        lax.fori_loop(0, pieces, one, 0)

        @pl.when(to_self(k))
        def _():
            sums_recv[mine, lax.rem(k, per_owner)] = sums[lax.rem(i, 2)]

        @pl.when(jnp.logical_not(to_self(k)))
        def _():
            sum_copy(i, k, mine).start()

    if units > 1:

        def take_all(i, carry):
            take_down(i)
            return carry

        lax.fori_loop(0, n, take_all, 0)

    def chunk_step(i, carry):
        @pl.when(i < chunks)
        def _():
            if units == 1:
                take_down(i)
            give_half(i)

        @pl.when(i >= 1)
        def _():
            sum_half(i - 1)

        return carry

    lax.fori_loop(0, chunks + 1, chunk_step, 0)

    group = sums_recv.shape[0]
    for source in range(group):
        for c in range(per_owner):

            @pl.when((source != mine) | (y != core))
            def _():
                sum_copy(0, c, source).wait_recv()

    def finish(p, carry):
        r = pl.ds(pl.multiple_of(p * tall, tall), tall)
        for c in range(per_owner):
            lanes = slice(c * width, (c + 1) * width)
            total = sums_recv[0, c, r].astype(jnp.float32)
            for source in range(1, group):
                total = total + sums_recv[source, c, r].astype(jnp.float32)
            own = stream[y, t, r, lanes].astype(jnp.float32)
            out_ref[r, lanes] = (own + 0.5 * total).astype(jnp.bfloat16)
        return carry

    lax.fori_loop(0, pieces, finish, 0)

    for i in range(max(chunks - 2, 0), chunks):
        last = chunk_at(i)
        give_copy(i, last).wait_send()

        @pl.when(jnp.logical_not(to_self(last)))
        def _():
            sum_copy(i, last, mine).wait_send()

    @pl.when(me < n - 1)
    def _():
        rim_copy.wait_send()

    def end_state(to, carry):
        state_copy(to, me).wait_send()
        return carry

    lax.fori_loop(me + 1, n, end_state, 0)

    def end_shares(b, carry):
        for buf, yy, send, fwd, recv in (
            (mix, 0, m_send, m_fwd, m_recv),
            (stream, y, r_send, r_fwd, r_recv),
        ):
            for d in range(nx):
                share(buf, yy, t, b, me, partner, send.at[d, b], recv).wait_send()
            for d in range(1, nx):
                share(buf, yy, t, b, me, partner, fwd.at[d, b], recv).wait_send()
        for d in range(nx):
            share(stream, y, t, b, me, partner, p_send.at[d, b], p_recv).wait_send()
            share(stream, y, t, b, me, partner, p_fwd.at[d, b], p_recv).wait_send()
        return carry

    lax.fori_loop(0, nb, end_shares, 0)

    def end_weights(s, carry):
        for w in range(3):
            @pl.when((s // 2 >= q) & (q > 0))
            def _():
                along(w, s, False).wait_send()

            @pl.when((s // 2 <= q) & (q < m - 1))
            def _():
                along(w, s, True).wait_send()

        return carry

    lax.fori_loop(0, n, end_weights, 0)
    for w in range(3):
        give_pair(w).wait_send()


def layer(x, gate, logs, step, taps, hgain, wout, residual, cgain, wg, wu, wd, heads, s1, s2):
    n, tp = lax.axis_size("sp"), lax.axis_size("tp")
    tokens, lanes = x.shape
    half = heads * HEAD
    cols = residual.shape[1]
    nb = tokens // BLOCK
    shard, units = wg.shape
    part = units // 2
    split = part % LANES != 0
    if split:
        wg, wu, wd = (w.reshape(shard, 2, part).swapaxes(0, 1) for w in (wg, wu, wd))
    width = max(shard, min(cols, 2 * LANES))
    chunks = tp * cols // width
    vmem = pl.BlockSpec(memory_space=pltpu.VMEM)
    hbm = pl.BlockSpec(memory_space=pl.ANY)
    dma = pltpu.SemaphoreType.DMA
    return pl.pallas_call(
        functools.partial(layer_kernel, n, tp, heads, s1, s2, split),
        out_shape=jax.ShapeDtypeStruct((tokens, cols), jnp.bfloat16),
        in_specs=[vmem] * 9 + [hbm] * 3,
        out_specs=vmem,
        scratch_shapes=[
            pltpu.VMEM((8, lanes), jnp.float32),
            pltpu.VMEM((RIM, lanes), jnp.bfloat16),
            pltpu.VMEM((tokens, 2 * half), jnp.bfloat16),
            pltpu.VMEM((tokens, 2 * (s1 + s2)), jnp.bfloat16),
            pltpu.VMEM((tokens, logs.shape[1]), jnp.float32),
            pltpu.VMEM((s1 + s2, half), jnp.float32),
            pltpu.VMEM((s1 + s2 + RIM, half), jnp.bfloat16),
            pltpu.VMEM((n, s1 + s2 + RIM, half), jnp.bfloat16),
            pltpu.VMEM((1, tp, tokens, 2 * half), jnp.bfloat16),
            pltpu.VMEM((2, tp, tokens, cols), jnp.bfloat16),
            pltpu.VMEM((2, tokens, tp * cols), jnp.bfloat16),
            pltpu.VMEM((3, n * shard, part), jnp.bfloat16),
            pltpu.VMEM((2, tokens, part), jnp.bfloat16),
            pltpu.VMEM((2, tokens, width), jnp.bfloat16),
            pltpu.VMEM((chunks, tokens, width), jnp.bfloat16),
            pltpu.VMEM((2, tokens, width), jnp.bfloat16),
            pltpu.VMEM((tp, cols // width, tokens, width), jnp.bfloat16),
            dma((2,)),
            dma((n,)),
            dma((n,)),
            dma((tp, nb)),
            dma((tp, nb)),
            dma((tp, nb)),
            dma((tp, nb)),
            dma((tp, nb)),
            dma((tp, nb)),
            dma((tp, nb)),
            dma((tp, nb)),
            dma((tp, nb)),
            dma((3,)),
            dma((3,)),
            dma((2, 3, n)),
            dma((3, n)),
            dma((2,)),
            dma((chunks,)),
            dma((2,)),
            dma((tp, cols // width)),
        ],
        compiler_params=pltpu.CompilerParams(
            has_side_effects=True, vmem_limit_bytes=VMEM_LIMIT
        ),
        name="layer",
    )(x, gate, logs, step, taps, hgain, wout, residual, cgain, wg, wu, wd)


def shards(
    grouped_head_inputs,
    head_gate_inputs,
    unsmoothed_step,
    head_decay_rate,
    extra_log_decay,
    first_group_keys,
    first_group_queries,
    second_group_keys,
    second_group_queries,
    head_input_filter,
    first_group_filter,
    second_group_filter,
    head_norm_gain,
    output_weight,
    residual,
    channel_norm_gain,
    channel_gate_weight,
    channel_up_weight,
    channel_down_weight,
):
    tp = lax.axis_size("tp")
    tokens = grouped_head_inputs.shape[0]
    heads = head_decay_rate.shape[1]
    half = heads * HEAD
    s1, s2 = first_group_keys.shape[1], second_group_keys.shape[1]
    x = jnp.concatenate(
        [
            grouped_head_inputs.reshape(tokens, 2 * half),
            first_group_keys,
            first_group_queries,
            second_group_keys,
            second_group_queries,
        ],
        axis=1,
    )
    taps = jnp.concatenate(
        [
            head_input_filter.reshape(CONV, 2 * half),
            first_group_filter.reshape(CONV, 2 * s1),
            second_group_filter.reshape(CONV, 2 * s2),
        ],
        axis=1,
    )
    step = jax.nn.softplus(unsmoothed_step.reshape(tokens, 2 * heads))
    logs = extra_log_decay.reshape(tokens, 2 * heads) - step * head_decay_rate.reshape(1, -1)
    pad = ((0, 0), (0, BLOCK - 2 * heads))
    wout = output_weight.reshape(2, tp, half, -1).swapaxes(0, 1).reshape(tp, 2 * half, -1)
    return layer(
        x,
        head_gate_inputs.reshape(tokens, 2 * half),
        jnp.pad(logs, pad),
        jnp.pad(step, pad),
        taps,
        head_norm_gain.reshape(1, 2 * half),
        wout,
        residual,
        channel_norm_gain.reshape(1, -1),
        channel_gate_weight,
        channel_up_weight,
        channel_down_weight,
        heads,
        s1,
        s2,
    )


def solution(mesh):
    return jax.shard_map(
        shards,
        mesh=mesh,
        in_specs=(
            P("sp", None, "tp"),
            P("sp", None, "tp"),
            P("sp", None, "tp"),
            P(None, "tp"),
            P("sp", None, "tp"),
            P("sp", None),
            P("sp", None),
            P("sp", None),
            P("sp", None),
            P(None, None, "tp"),
            P(),
            P(),
            P(None, "tp"),
            P(None, None, "tp"),
            P("sp", "tp"),
            P(),
            P("sp", "tp"),
            P("sp", "tp"),
            P("sp", "tp"),
        ),
        out_specs=P("sp", "tp"),
        check_vma=False,
    )
```

profile of v0, /device:TPU:28, one launch (start us, length us, event | category | flops | bytes accessed | tf_op | source)
XLA Modules:
  0.0 273.0 jit_solution(3538156941717540394)
XLA Ops:
  0.0 0.8 mul.10
  0.8 0.8 reshape.41
  1.5 1.2 copy.51
  2.8 0.7 copy.53
  3.5 0.7 copy.49
  4.2 0.6 pad_maximum_fusion.taps_ref
  4.8 0.8 reshape.38
  5.5 0.8 reshape.37
  6.3 1.1 copy.34
  7.4 1.7 copy.35
  9.2 0.2 copy.43
  9.4 0.2 copy.36
  9.6 0.0 copy-start.1
  9.6 0.3 compare_select_fusion
  9.9 0.9 pad.8.step_ref
  10.8 0.8 pad.7.log_ref
  11.6 0.0 copy-done.1
  11.6 0.2 copy.47
  11.8 0.0 copy-start
  11.8 3.7 %concatenate.6.x_ref = bf16[1024,896]{1,0:T(8,128)(2,1)} concatenate(bf16[1024,512]{1,0:T(8,128)(2,1)S(1)} %bitcast.23, bf16[1024,128]{1,0:T(8,128)(2,1)} %param.24, bf16[1024,128]{1,0:T(8,128)(2,1)} %param.25, bf16[1024,64]{1,0:T(8,128)(2,1)S(1)} %copy.34, bf16[1024,64]{1,0:T(8,128)(2,1)} %copy.35), dimensions={1} | concatenate | bytes 3670016 | tf_op jit(solution)/shard_map/concatenate | solution.py:733
  15.6 2.4 copy.48
  18.0 1.6 copy.44
  19.6 251.2 %layer.1 = bf16[1024,512]{1,0:T(8,128)(2,1)} custom-call(bf16[1024,896]{1,0:T(8,128)(2,1)} %concatenate.6.x_ref, bf16[1024,512]{1,0:T(8,128)(2,1)} %bitcast.24, f32[1024,128]{1,0:T(8,128)} %pad.7.log_ref, f32[1024,128]{1,0:T(8,128)} %pad.8.step_ref, f32[4,896]{1,0:T(4,128)} %pad_maximum_fusion.taps_ref, f32[1,512]{1,0:T(1,128)} %bitcast.32, ...), custom_call_target="tpu_custom_call" | custom-call | tf_op jit(solution)/shard_map/layer/pallas_call | solution.py:656
  270.8 2.3 copy.55
  (1 shorter events, 0.0 us)
Async XLA Ops:
  9.6 2.0 copy-start.1
  11.8 6.2 %copy-start = (bf16[2,1024,512]{2,1,0:T(8,128)(2,1)S(1)}, bf16[2,1024,512]{2,1,0:T(8,128)(2,1)}, u32[]{:S(2)}) copy-start(bf16[2,1024,512]{2,1,0:T(8,128)(2,1)} %param.32) | copy-start | bytes 6291460
where the time goes:
time: 275 us; the launch traced here: 273 us
  Pallas kernels  251 us (91%)
  local copies, waits for them, and re-layouts  20.8 us (8%)
    pallas_call x1, Pallas kernels, layer(): pl.pallas_call(functools.partial(layer_kernel, n, tp, heads, s1, s2, spli...  251 us
    unnamed x12, local copies, waits for them, and re-layouts  10.4 us

commit v1 on v0

--- a/solution.py
+++ b/solution.py
@@ -35,13 +35,15 @@
 
 def layer_kernel(
     n, tp, heads, s1, s2, split,
-    x_ref, gate_ref, log_ref, step_ref, taps_ref, hgain_ref, wout_ref, res_ref, cgain_ref,
-    wg_ref, wu_ref, wd_ref,
+    x_ref, keys1_ref, queries1_ref, keys2_ref, queries2_ref, unsmoothed_ref, extra_ref, rate_ref,
+    head_taps_ref, taps1_ref, taps2_ref, hgain_ref, cgain_ref,
+    gate_in, wout_in, res_in, wg_ref, wu_ref, wd_ref,
     out_ref,
-    xs, rim, vals, kq, cums, st, stsend, strecv, mix, stream, normed, weights, hidden,
-    give, give_recv, sums, sums_recv,
+    gate_ref, wout_ref, res_ref, in_sems, taps_ref, step_rows, log_rows, rim_out, xs, rim, vals, kq, cums, st, stsend, strecv, mix, stream, normed, weights, hidden,
+    give, give_recv, sums, across_recv, ready, sums_recv,
     rim_sems, st_send, st_recv, m_send, m_fwd, m_recv, r_send, r_fwd, r_recv,
-    p_send, p_fwd, p_recv, w_local, w_pair, w_send, w_recv, g_send, g_recv, s_send, s_recv,
+    p_send, p_fwd, p_recv, w_local, w_pair, w_send, w_recv,
+    g_send, g_recv, a_send, a_recv, s_send, s_recv,
 ):
     me = lax.axis_index("sp")
     t = lax.axis_index("tp")
@@ -105,47 +107,68 @@
         for w in range(2):
             give_pair(w).start()
             send_along(w, me, False, own=True)
-            send_along(w, me, True, own=True)
-        give_pair(2).start()
+        send_along(0, me, True, own=True)
         for w in range(3):
             keep_own(w).start()
 
-    def relay(w, d, sel):
-        other = lax.rem(y + sel, 2)
+    def relay_down(k):
+        w, d, sel = lax.rem(k, 2), k // 4, lax.rem(k // 2, 2)
 
         @pl.when(q + d < m)
         def _():
-            s = (q + d) * 2 + other
+            s = (q + d) * 2 + lax.rem(y + sel, 2)
             take_unit(w, s)
             send_along(w, s, False)
 
-            @pl.when(d == 0)
-            def _():
-                send_along(w, s, True)
-
-        @pl.when((d > 0) & (q - d >= 0))
-        def _():
-            s = (q - d) * 2 + other
+    def relay_up(k):
+        w, d, sel = lax.rem(k, 2), k // 4, lax.rem(k // 2, 2)
+
+        @pl.when(q - d >= 0)
+        def _():
+            s = (q - d) * 2 + lax.rem(y + sel, 2)
             take_unit(w, s)
             send_along(w, s, True)
 
-    def relay_step(k):
-        relay(lax.rem(k, 2), k // 4, lax.rem(k // 2, 2))
-
     early = 4 * (m - 1)
-    points = nb // 2 + (nb + 4) // 2
-    per_point = pl.cdiv(max(early - 2, 0), points)
-
-    def relay_point(p):
-        for i in range(per_point):
-            k = 2 + p * per_point + i
-
-            @pl.when(k < early)
-            def _():
-                relay_step(k)
+    stride = max(m - 3, 0)
+
+    def relay_points(b, first, go):
+        for j, at in enumerate((0, 1, 3, 4)):
+
+            @pl.when(b == first + at)
+            def _():
+                if m > 2:
+                    go(4 + j)
+
+        for j in range(4):
+
+            @pl.when(b == first + nb - 2 + j)
+            def _():
+                for i in range(stride):
+                    go(8 + j * stride + i)
+
+    later = [
+        pltpu.make_async_copy(source, place, in_sems.at[i])
+        for i, (source, place) in enumerate(
+            ((gate_in, gate_ref), (wout_in, wout_ref), (res_in, res_ref))
+        )
+    ]
+
+    def tokens_of(b):
+        r = rows_of(b)
+        second = jnp.concatenate([keys2_ref[:, r], queries2_ref[:, r]], axis=0)
+        return jnp.concatenate(
+            [
+                x_ref[r].astype(jnp.float32),
+                keys1_ref[r].astype(jnp.float32),
+                queries1_ref[r].astype(jnp.float32),
+                second.astype(jnp.float32).T,
+            ],
+            axis=1,
+        )
 
     rim_copy = pltpu.make_async_remote_copy(
-        src_ref=x_ref.at[pl.ds(x_ref.shape[0] - RIM, RIM)],
+        src_ref=rim_out,
         dst_ref=rim,
         send_sem=rim_sems.at[0],
         recv_sem=rim_sems.at[1],
@@ -153,11 +176,31 @@
         device_id_type=MESH,
     )
 
+    start_weights()
+
     @pl.when(me < n - 1)
     def _():
+        rim_out[...] = tokens_of(nb - 1)[BLOCK - RIM :].astype(jnp.bfloat16)
         rim_copy.start()
 
-    start_weights()
+    for copy in later:
+        copy.start()
+
+    for g in range(2):
+        taps_ref[:, g * half : (g + 1) * half] = head_taps_ref[:, g, :]
+        taps_ref[:, wide + g * s1 : wide + (g + 1) * s1] = taps1_ref[:, g, :]
+    taps_ref[:, wide + 2 * s1 :] = jnp.concatenate([taps2_ref[:, 0, :], taps2_ref[:, 1, :]], axis=1)
+
+    unsmoothed = unsmoothed_ref[...]
+    steps = jnp.maximum(unsmoothed, 0.0) + jnp.log1p(jnp.exp(-jnp.abs(unsmoothed)))
+    step_rows[...] = jnp.zeros_like(step_rows)
+    log_rows[...] = jnp.zeros_like(log_rows)
+    for g in range(2):
+        for h in range(heads):
+            c = g * heads + h
+            row = steps[g, h : h + 1]
+            step_rows[c : c + 1] = row
+            log_rows[c : c + 1] = extra_ref[g, h : h + 1] - row * rate_ref[g, h]
 
     @pl.when(me > 0)
     def _():
@@ -172,7 +215,8 @@
     row_i = lax.broadcasted_iota(jnp.int32, (BLOCK, BLOCK), 0)
     col_i = lax.broadcasted_iota(jnp.int32, (BLOCK, BLOCK), 1)
     causal = row_i >= col_i
-    tri = jnp.where(causal, 1.0, 0.0).astype(jnp.float32)
+    tri = jnp.where(row_i <= col_i, 1.0, 0.0).astype(jnp.float32)
+    rows8 = log_rows.shape[0]
 
     def state_update(b, cum):
         last = cum[BLOCK - 1 : BLOCK]
@@ -194,7 +238,7 @@
 
     def first_pass(b, total):
         r = rows_of(b)
-        current = x_ref[r].astype(jnp.float32)
+        current = tokens_of(b)
         taps = taps_ref[...]
         extended = jnp.concatenate([xs[...], current], axis=0)
         acc = taps[CONV - 1 : CONV] * current
@@ -202,33 +246,39 @@
             acc = acc + taps[k : k + 1] * pltpu.roll(extended, CONV - 1 - k, 0)[8:]
         xs[...] = current[BLOCK - 8 :]
         acc = acc * sigmoid(acc)
-        vals[r] = (acc[:, :wide] * spread(step_ref[r], 0, 2 * heads)).astype(jnp.bfloat16)
+        cum_rows = jnp.dot(
+            log_rows[:, r], tri, precision=lax.Precision.HIGHEST, preferred_element_type=jnp.float32
+        )
+        fill = jnp.zeros((BLOCK - 2 * rows8, BLOCK), jnp.float32)
+        cum = jnp.concatenate([cum_rows, step_rows[:, r], fill], axis=0).T
+        cums[r] = cum
+        vals[r] = (acc[:, :wide] * spread(cum, rows8, 2 * heads)).astype(jnp.bfloat16)
         kq[r] = acc[:, wide:].astype(jnp.bfloat16)
-        cum = jnp.dot(
-            tri, log_ref[r], precision=lax.Precision.HIGHEST, preferred_element_type=jnp.float32
-        )
-        cums[r] = cum
         state_update(b, cum)
 
-        @pl.when(lax.rem(b, 2) == 1)
-        def _():
-            relay_point(b // 2)
-
         return total + cum[BLOCK - 1 : BLOCK]
 
-    total = lax.fori_loop(0, nb, first_pass, jnp.zeros((1, log_ref.shape[1]), jnp.float32))
+    total = lax.fori_loop(0, nb, first_pass, jnp.zeros((1, BLOCK), jnp.float32))
 
     states = s1 + s2
-    stsend[0:states] = st[...].astype(jnp.bfloat16)
-    which = lax.broadcasted_iota(jnp.int32, (RIM, half), 0)
-    extra = jnp.zeros((RIM, half), jnp.float32)
-    for g in range(2):
-        logs = spread(total, g * heads, heads)
-        high = logs.astype(jnp.bfloat16).astype(jnp.float32)
-        low = logs - high
-        extra = jnp.where(which == g, high, extra)
-        extra = jnp.where(which == 2 + g, low, extra)
-    stsend[states : states + RIM] = extra.astype(jnp.bfloat16)
+
+    def pack_state(total):
+        stsend[0:states] = st[...].astype(jnp.bfloat16)
+        which = lax.broadcasted_iota(jnp.int32, (RIM, half), 0)
+        extra = jnp.zeros((RIM, half), jnp.float32)
+        for g in range(2):
+            logs = total[g]
+            high = logs.astype(jnp.bfloat16).astype(jnp.float32)
+            low = logs - high
+            extra = jnp.where(which == g, high, extra)
+            extra = jnp.where(which == 2 + g, low, extra)
+        stsend[states : states + RIM] = extra.astype(jnp.bfloat16)
+
+    def logs_of(got):
+        return [
+            got[states + g : states + g + 1] + got[states + 2 + g : states + 3 + g]
+            for g in range(2)
+        ]
 
     def state_copy(to, source):
         return pltpu.make_async_remote_copy(
@@ -244,19 +294,53 @@
         state_copy(to, me).start()
         return carry
 
-    lax.fori_loop(me + 1, n, send_state, 0)
-    st[...] = jnp.zeros_like(st)
-
-    def take_state(source, carry):
-        state_copy(n - 1, source).wait_recv()
-        got = strecv[source].astype(jnp.float32)
+    own_logs = [spread(total, g * heads, heads) for g in range(2)]
+
+    @pl.when(y == 0)
+    def _():
+        pack_state(own_logs)
+        state_copy(pair, me).start()
+
+    @pl.when(y == 1)
+    def _():
+        state_copy(me, pair).wait_recv()
+        got = strecv[pair].astype(jnp.float32)
         for g in range(2):
             base, size = (0, s1) if g == 0 else (s1, s2)
-            logs = got[states + g : states + g + 1] + got[states + 2 + g : states + 3 + g]
-            st[base : base + size] = st[base : base + size] * jnp.exp(logs) + got[base : base + size]
-        return carry
-
-    lax.fori_loop(0, me, take_state, 0)
+            st[base : base + size] = (
+                st[base : base + size] + got[base : base + size] * jnp.exp(own_logs[g])
+            )
+        both = [a + b for a, b in zip(logs_of(got), own_logs)]
+        pack_state(both)
+        lax.fori_loop(me + 1, n, send_state, 0)
+
+    send_along(1, me, True, own=True)
+    for w in range(2):
+        take_unit(w, pair)
+        send_along(w, pair, False)
+        send_along(w, pair, True)
+    st[...] = jnp.zeros_like(st)
+
+    def add_state(source):
+        got = strecv[source].astype(jnp.float32)
+        logs = logs_of(got)
+        for g in range(2):
+            base, size = (0, s1) if g == 0 else (s1, s2)
+            st[base : base + size] = (
+                st[base : base + size] * jnp.exp(logs[g]) + got[base : base + size]
+            )
+
+    def take_state(before, carry):
+        source = before * 2 + 1
+        state_copy(n - 1, source).wait_recv()
+        add_state(source)
+        return carry
+
+    lax.fori_loop(0, q, take_state, 0)
+
+    @pl.when(y == 1)
+    def _():
+        add_state(pair)
 
     def share(buf, yy, source, b, sp, to, send, recv):
         piece = buf.at[yy, source, rows_of(b)]
@@ -292,9 +376,7 @@
             share(buf, yy, source, b, me, partner, send.at[0, b], recv).wait_recv()
 
     def send_pair(b):
-        for d in range(nx):
-            to = across(d) + core
-            share(stream, y, t, b, pair, to, p_send.at[d, b], p_recv).start()
+        share(stream, y, t, b, pair, t, p_send.at[0, b], p_recv).start()
 
     def forward_pair(b):
         for d in range(nx):
@@ -340,7 +422,7 @@
                 y = y * (z * sigmoid(z))
                 y = y * lax.rsqrt(jnp.mean(y * y, axis=1, keepdims=True) + EPSILON)
                 outs.append(y)
-            out = jnp.concatenate(outs, axis=1) * hgain_ref[:, g * half : (g + 1) * half]
+            out = jnp.concatenate(outs, axis=1) * hgain_ref[g : g + 1]
             mix[0, t, r, g * half : (g + 1) * half] = out.astype(jnp.bfloat16)
         state_update(b, cum)
         send_own(mix, 0, b, m_send, m_recv)
@@ -350,9 +432,12 @@
         wait_rest(mix, 0, b, m_send, m_recv)
         acc = res_ref[r].astype(jnp.float32)
         for source in range(tp):
-            acc = acc + jnp.dot(
-                mix[0, source, r], wout_ref[source], preferred_element_type=jnp.float32
-            )
+            for g in range(2):
+                acc = acc + jnp.dot(
+                    mix[0, source, r, g * half : (g + 1) * half],
+                    wout_ref[g, source * half : (source + 1) * half],
+                    preferred_element_type=jnp.float32,
+                )
         stream[y, t, r] = acc.astype(jnp.bfloat16)
         send_own(stream, y, b, r_send, r_recv)
         send_pair(b)
@@ -370,14 +455,15 @@
                 jnp.bfloat16
             )
 
+    down = 2
+
     def stage(b, carry):
         @pl.when(b < nb)
         def _():
             second_pass(b)
 
-        @pl.when(lax.rem(b, 2) == 0)
-        def _():
-            relay_point(nb // 2 + b // 2)
+        relay_points(b, 0, relay_down)
+        relay_points(b, 1, relay_up)
 
         @pl.when((b >= 1) & (b < nb + 1))
         def _():
@@ -387,35 +473,72 @@
         def _():
             project(b - 2)
 
+        @pl.when(b == nb)
+        def _():
+            give_pair(2).start()
+
+        @pl.when(b == nb + 3)
+        def _():
+            send_along(down, me, False, own=True)
+            send_along(down, me, True, own=True)
+
         @pl.when((b >= 3) & (b < nb + 3))
         def _():
             forward(stream, y, b - 3, r_fwd, r_recv)
-            forward_pair(b - 3)
-
-        @pl.when(b >= 4)
+            for d in range(1, nx):
+                source = across(d) + core
+                share(stream, y, source, b - 3, pair, t, p_send.at[d, b - 3], p_recv).start()
+
+        @pl.when((b >= 4) & (b < nb + 4))
         def _():
             wait_rest(stream, y, b - 4, r_send, r_recv)
             normalise(y, b - 4)
-            wait_pair(b - 4)
-            normalise(1 - y, b - 4)
-
-        return carry
-
-    lax.fori_loop(0, nb + 4, stage, 0)
-
-    down = 2
-    send_along(down, me, False, own=True)
-    send_along(down, me, True, own=True)
+
+        @pl.when((b >= 6) & (b < nb + 6))
+        def _():
+            forward_pair(b - 6)
+
+        @pl.when(b >= 7)
+        def _():
+            wait_pair(b - 7)
+            normalise(1 - y, b - 7)
+
+        return carry
+
+    for copy in later:
+        copy.wait()
+    lax.fori_loop(0, nb + 7, stage, 0)
+
+    between = (q > 0) & (q < m - 1)
+
+    def relay_far(d):
+        for sel in range(2):
+
+            @pl.when(between & (q + d < m))
+            def _():
+                s = (q + d) * 2 + sel
+                take_unit(down, s)
+                send_along(down, s, False)
+
+            @pl.when(between & (q - d >= 0))
+            def _():
+                s = (q - d) * 2 + sel
+                take_unit(down, s)
+                send_along(down, s, True)
+
+    keep_own(down).wait()
     take_unit(down, pair)
     send_along(down, pair, False)
     send_along(down, pair, True)
+    relay_far(1)
 
     def late(k, carry):
-        relay_step(k)
-        return carry
-
-    lax.fori_loop(early, 4 * m, late, 0)
-    for w in range(3):
+        relay_down(k)
+        relay_up(k)
+        return carry
+
+    lax.fori_loop(max(early, 4), 4 * m, late, 0)
+    for w in range(2):
         keep_own(w).wait()
 
     tall = 2 * BLOCK
@@ -432,6 +555,12 @@
 
     lax.fori_loop(0, 2 * pieces, mix_channels, 0)
 
+    def pass_on(d, carry):
+        relay_far(d)
+        return carry
+
+    lax.fori_loop(2, m, pass_on, 0)
+
     near = jnp.minimum(q, m - 1 - q)
 
     def block_at(i):
@@ -446,22 +575,12 @@
     per_owner = cols // width
 
     def shard_at(i):
-        return block_at(i // 2) * 2 + lax.rem(y + lax.rem(i, 2), 2)
+        return block_at(i // 2) * 2 + lax.rem(i, 2)
 
     def take_down(i):
-        s = shard_at(i)
-
-        @pl.when(i >= 2)
-        def _():
-            take_unit(down, s)
-
-            @pl.when(s > me)
-            def _():
-                send_along(down, s, False)
-
-            @pl.when(s < me)
-            def _():
-                send_along(down, s, True)
+        @pl.when((i >= 2) & jnp.logical_not(between))
+        def _():
+            take_unit(down, shard_at(i))
 
     def chunk_at(i):
         return shard_at(i) if units == 1 else i
@@ -473,74 +592,104 @@
             hidden[yy, r], block, (((1,), (1,)), ((), ())), preferred_element_type=jnp.float32
         )
 
-    def give_copy(i, k):
+    def rows_at(p):
+        return pl.ds(pl.multiple_of(p * tall, tall), tall)
+
+    def give_copy(i, k, p):
         return pltpu.make_async_remote_copy(
-            src_ref=give.at[lax.rem(i, 2)],
-            dst_ref=give_recv.at[k],
-            send_sem=g_send.at[lax.rem(i, 2)],
-            recv_sem=g_recv.at[k],
+            src_ref=give.at[lax.rem(i, 2), rows_at(p)],
+            dst_ref=give_recv.at[k, rows_at(p)],
+            send_sem=g_send.at[lax.rem(i, 2), p],
+            recv_sem=g_recv.at[k, p],
             device_id={"tp": partner},
             device_id_type=MESH,
         )
 
-    mine = my_x * 2 + y
-
-    def sum_copy(i, k, source):
+    def pair_copy(i, k, p):
         return pltpu.make_async_remote_copy(
-            src_ref=sums.at[lax.rem(i, 2)],
-            dst_ref=sums_recv.at[source, lax.rem(k, per_owner)],
-            send_sem=s_send.at[lax.rem(i, 2)],
-            recv_sem=s_recv.at[source, lax.rem(k, per_owner)],
-            device_id={"sp": q * 2 + core, "tp": k // per_owner},
+            src_ref=sums.at[lax.rem(i, 2), rows_at(p)],
+            dst_ref=across_recv.at[k, rows_at(p)],
+            send_sem=a_send.at[lax.rem(i, 2), p],
+            recv_sem=a_recv.at[k, p],
+            device_id={"sp": pair},
             device_id_type=MESH,
         )
 
-    def to_self(k):
-        return (k // per_owner == t) & (y == core)
+    def owner_copy(i, k, p, source):
+        return pltpu.make_async_remote_copy(
+            src_ref=ready.at[lax.rem(i, 2), rows_at(p)],
+            dst_ref=sums_recv.at[source, lax.rem(k, per_owner), rows_at(p)],
+            send_sem=s_send.at[lax.rem(i, 2), p],
+            recv_sem=s_recv.at[source, lax.rem(k, per_owner), p],
+            device_id={"tp": k // per_owner},
+            device_id_type=MESH,
+        )
+
+    keeps = core == y
 
     def give_half(i):
         k = chunk_at(i)
 
-        @pl.when(i >= 2)
-        def _():
-            give_copy(i, k).wait_send()
-
         def one(p, carry):
-            r = pl.ds(pl.multiple_of(p * tall, tall), tall)
-            give[lax.rem(i, 2), r] = product(1 - core, k, p).astype(jnp.bfloat16)
+            @pl.when(i >= 2)
+            def _():
+                give_copy(i, k, p).wait_send()
+
+            give[lax.rem(i, 2), rows_at(p)] = product(1 - core, k, p).astype(jnp.bfloat16)
+            give_copy(i, k, p).start()
             return carry
 
         lax.fori_loop(0, pieces, one, 0)
-        give_copy(i, k).start()
 
     def sum_half(i):
         k = chunk_at(i)
 
-        @pl.when(i >= 2)
-        def _():
-            before = chunk_at(i - 2)
-
-            @pl.when(jnp.logical_not(to_self(before)))
-            def _():
-                sum_copy(i, before, mine).wait_send()
-
-        give_copy(i, k).wait_recv()
-
         def one(p, carry):
-            r = pl.ds(pl.multiple_of(p * tall, tall), tall)
-            both = product(core, k, p) + give_recv[k, r].astype(jnp.float32)
-            sums[lax.rem(i, 2), r] = both.astype(jnp.bfloat16)
+            @pl.when(jnp.logical_not(keeps) & (i >= 2))
+            def _():
+                pair_copy(i, k, p).wait_send()
+
+            give_copy(i, k, p).wait_recv()
+            both = product(core, k, p) + give_recv[k, rows_at(p)].astype(jnp.float32)
+            sums[lax.rem(i, 2), rows_at(p)] = both.astype(jnp.bfloat16)
+
+            @pl.when(jnp.logical_not(keeps))
+            def _():
+                pair_copy(i, k, p).start()
+
             return carry
 
         lax.fori_loop(0, pieces, one, 0)
 
-        @pl.when(to_self(k))
-        def _():
-            sums_recv[mine, lax.rem(k, per_owner)] = sums[lax.rem(i, 2)]
-
-        @pl.when(jnp.logical_not(to_self(k)))
-        def _():
-            sum_copy(i, k, mine).start()
+    def sum_pair(i):
+        k = chunk_at(i)
+        away = k // per_owner != t
+        before = chunk_at(jnp.maximum(i - 2, 0))
+
+        def one(p, carry):
+            @pl.when((i >= 2) & (before // per_owner != t))
+            def _():
+                owner_copy(i, before, p, my_x).wait_send()
+
+            pair_copy(i, k, p).wait_recv()
+            r = rows_at(p)
+            both = sums[lax.rem(i, 2), r].astype(jnp.float32) + across_recv[k, r].astype(
+                jnp.float32
+            )
+            both = both.astype(jnp.bfloat16)
+
+            @pl.when(away)
+            def _():
+                ready[lax.rem(i, 2), r] = both
+                owner_copy(i, k, p, my_x).start()
+
+            @pl.when(jnp.logical_not(away))
+            def _():
+                sums_recv[my_x, lax.rem(k, per_owner), r] = both
+
+            return carry
+
+        lax.fori_loop(0, pieces, one, 0)
 
     if units > 1:
 
@@ -557,28 +706,30 @@
                 take_down(i)
             give_half(i)
 
-        @pl.when(i >= 1)
+        @pl.when((i >= 1) & (i < chunks + 1))
         def _():
             sum_half(i - 1)
 
-        return carry
-
-    lax.fori_loop(0, chunks + 1, chunk_step, 0)
-
-    group = sums_recv.shape[0]
-    for source in range(group):
+        @pl.when(keeps & (i >= 2))
+        def _():
+            sum_pair(i - 2)
+
+        return carry
+
+    lax.fori_loop(0, chunks + 2, chunk_step, 0)
+
+    def finish(p, carry):
+        r = rows_at(p)
         for c in range(per_owner):
-
-            @pl.when((source != mine) | (y != core))
-            def _():
-                sum_copy(0, c, source).wait_recv()
-
-    def finish(p, carry):
-        r = pl.ds(pl.multiple_of(p * tall, tall), tall)
-        for c in range(per_owner):
+            for source in range(nx):
+
+                @pl.when((source != my_x) | jnp.logical_not(keeps))
+                def _():
+                    owner_copy(0, c, p, source).wait_recv()
+
             lanes = slice(c * width, (c + 1) * width)
             total = sums_recv[0, c, r].astype(jnp.float32)
-            for source in range(1, group):
+            for source in range(1, nx):
                 total = total + sums_recv[source, c, r].astype(jnp.float32)
             own = stream[y, t, r, lanes].astype(jnp.float32)
             out_ref[r, lanes] = (own + 0.5 * total).astype(jnp.bfloat16)
@@ -586,13 +737,22 @@
 
     lax.fori_loop(0, pieces, finish, 0)
 
-    for i in range(max(chunks - 2, 0), chunks):
-        last = chunk_at(i)
-        give_copy(i, last).wait_send()
-
-        @pl.when(jnp.logical_not(to_self(last)))
-        def _():
-            sum_copy(i, last, mine).wait_send()
+    def end_sums(p, carry):
+        for i in range(max(chunks - 2, 0), chunks):
+            last = chunk_at(i)
+            give_copy(i, last, p).wait_send()
+
+            @pl.when(jnp.logical_not(keeps))
+            def _():
+                pair_copy(i, last, p).wait_send()
+
+            @pl.when(keeps & (last // per_owner != t))
+            def _():
+                owner_copy(i, last, p, my_x).wait_send()
+
+        return carry
+
+    lax.fori_loop(0, pieces, end_sums, 0)
 
     @pl.when(me < n - 1)
     def _():
@@ -602,7 +762,7 @@
         state_copy(to, me).wait_send()
         return carry
 
-    lax.fori_loop(me + 1, n, end_state, 0)
+    lax.fori_loop(me + 1, jnp.where(y == 0, me + 2, n), end_state, 0)
 
     def end_shares(b, carry):
         for buf, yy, send, fwd, recv in (
@@ -637,10 +797,13 @@
         give_pair(w).wait_send()
 
 
-def layer(x, gate, logs, step, taps, hgain, wout, residual, cgain, wg, wu, wd, heads, s1, s2):
+def layer(front, later, wg, wu, wd, heads, s1, s2):
     n, tp = lax.axis_size("sp"), lax.axis_size("tp")
-    tokens, lanes = x.shape
+    gate, wout, residual = later
+    tokens = gate.shape[0]
     half = heads * HEAD
+    lanes = 2 * (half + s1 + s2)
+    rows8 = -(-2 * heads // 8) * 8
     cols = residual.shape[1]
     nb = tokens // BLOCK
     shard, units = wg.shape
@@ -650,20 +813,32 @@
         wg, wu, wd = (w.reshape(shard, 2, part).swapaxes(0, 1) for w in (wg, wu, wd))
     width = max(shard, min(cols, 2 * LANES))
     chunks = tp * cols // width
+    pieces = tokens // (2 * BLOCK)
     vmem = pl.BlockSpec(memory_space=pltpu.VMEM)
     hbm = pl.BlockSpec(memory_space=pl.ANY)
     dma = pltpu.SemaphoreType.DMA
     return pl.pallas_call(
         functools.partial(layer_kernel, n, tp, heads, s1, s2, split),
         out_shape=jax.ShapeDtypeStruct((tokens, cols), jnp.bfloat16),
-        in_specs=[vmem] * 9 + [hbm] * 3,
+        in_specs=[vmem] * 7
+        + [pl.BlockSpec(memory_space=pltpu.SMEM)]
+        + [vmem] * 5
+        + [hbm] * 6,
         out_specs=vmem,
         scratch_shapes=[
+            pltpu.VMEM(gate.shape, gate.dtype),
+            pltpu.VMEM(wout.shape, wout.dtype),
+            pltpu.VMEM(residual.shape, residual.dtype),
+            dma((3,)),
+            pltpu.VMEM((CONV, lanes), jnp.float32),
+            pltpu.VMEM((rows8, tokens), jnp.float32),
+            pltpu.VMEM((rows8, tokens), jnp.float32),
+            pltpu.VMEM((RIM, lanes), jnp.bfloat16),
             pltpu.VMEM((8, lanes), jnp.float32),
             pltpu.VMEM((RIM, lanes), jnp.bfloat16),
             pltpu.VMEM((tokens, 2 * half), jnp.bfloat16),
             pltpu.VMEM((tokens, 2 * (s1 + s2)), jnp.bfloat16),
-            pltpu.VMEM((tokens, logs.shape[1]), jnp.float32),
+            pltpu.VMEM((tokens, BLOCK), jnp.float32),
             pltpu.VMEM((s1 + s2, half), jnp.float32),
             pltpu.VMEM((s1 + s2 + RIM, half), jnp.bfloat16),
             pltpu.VMEM((n, s1 + s2 + RIM, half), jnp.bfloat16),
@@ -675,7 +850,9 @@
             pltpu.VMEM((2, tokens, width), jnp.bfloat16),
             pltpu.VMEM((chunks, tokens, width), jnp.bfloat16),
             pltpu.VMEM((2, tokens, width), jnp.bfloat16),
-            pltpu.VMEM((tp, cols // width, tokens, width), jnp.bfloat16),
+            pltpu.VMEM((chunks, tokens, width), jnp.bfloat16),
+            pltpu.VMEM((2, tokens, width), jnp.bfloat16),
+            pltpu.VMEM((tp // 2, cols // width, tokens, width), jnp.bfloat16),
             dma((2,)),
             dma((n,)),
             dma((n,)),
@@ -692,16 +869,18 @@
             dma((3,)),
             dma((2, 3, n)),
             dma((3, n)),
-            dma((2,)),
-            dma((chunks,)),
-            dma((2,)),
-            dma((tp, cols // width)),
+            dma((2, pieces)),
+            dma((chunks, pieces)),
+            dma((2, pieces)),
+            dma((chunks, pieces)),
+            dma((2, pieces)),
+            dma((tp // 2, cols // width, pieces)),
         ],
         compiler_params=pltpu.CompilerParams(
             has_side_effects=True, vmem_limit_bytes=VMEM_LIMIT
         ),
         name="layer",
-    )(x, gate, logs, step, taps, hgain, wout, residual, cgain, wg, wu, wd)
+    )(*front, gate, wout, residual, wg, wu, wd)
 
 
 def shards(
@@ -725,43 +904,27 @@
     channel_up_weight,
     channel_down_weight,
 ):
-    tp = lax.axis_size("tp")
     tokens = grouped_head_inputs.shape[0]
     heads = head_decay_rate.shape[1]
     half = heads * HEAD
     s1, s2 = first_group_keys.shape[1], second_group_keys.shape[1]
-    x = jnp.concatenate(
-        [
+    return layer(
+        (
             grouped_head_inputs.reshape(tokens, 2 * half),
             first_group_keys,
             first_group_queries,
-            second_group_keys,
-            second_group_queries,
-        ],
-        axis=1,
-    )
-    taps = jnp.concatenate(
-        [
-            head_input_filter.reshape(CONV, 2 * half),
-            first_group_filter.reshape(CONV, 2 * s1),
-            second_group_filter.reshape(CONV, 2 * s2),
-        ],
-        axis=1,
-    )
-    step = jax.nn.softplus(unsmoothed_step.reshape(tokens, 2 * heads))
-    logs = extra_log_decay.reshape(tokens, 2 * heads) - step * head_decay_rate.reshape(1, -1)
-    pad = ((0, 0), (0, BLOCK - 2 * heads))
-    wout = output_weight.reshape(2, tp, half, -1).swapaxes(0, 1).reshape(tp, 2 * half, -1)
-    return layer(
-        x,
-        head_gate_inputs.reshape(tokens, 2 * half),
-        jnp.pad(logs, pad),
-        jnp.pad(step, pad),
-        taps,
-        head_norm_gain.reshape(1, 2 * half),
-        wout,
-        residual,
-        channel_norm_gain.reshape(1, -1),
+            second_group_keys.T,
+            second_group_queries.T,
+            unsmoothed_step.transpose(1, 2, 0),
+            extra_log_decay.transpose(1, 2, 0),
+            head_decay_rate,
+            head_input_filter,
+            first_group_filter,
+            second_group_filter,
+            head_norm_gain,
+            channel_norm_gain.reshape(1, -1),
+        ),
+        (head_gate_inputs.reshape(tokens, 2 * half), output_weight, residual),
         channel_gate_weight,
         channel_up_weight,
         channel_down_weight,

time: 275 us -> 207 us (0.75)
  the two profiles are of different devices: /device:TPU:28 before, /device:TPU:24 now
where the time goes in v1:
time: 207 us
  Pallas kernels  201 us (97%)
  local copies, waits for them, and re-layouts  5.99 us (3%)
    pallas_call x1, Pallas kernels, layer(): pl.pallas_call(functools.partial(layer_kernel, n, tp, heads, s1, s2, spli...  201 us
    unnamed x5, local copies, waits for them, and re-layouts  5.99 us

profile of v1, /device:TPU:24, one launch (start us, length us, event | category | flops | bytes accessed | tf_op | source)
XLA Modules:
  0.0 206.9 jit_solution(3328546340890907056)
XLA Ops:
  0.0 0.0 copy-start
  0.0 2.5 %copy.20 = bf16[128,8,2,256]{3,1,2,0:T(8,128)(2,1)} copy(bf16[128,8,2,256]{3,2,1,0:T(2,128)(2,1)} %bitcast.11) | data formatting | bytes 2097152
  2.5 0.0 copy-done
  2.5 1.2 copy.21
  3.7 200.9 %layer.1 = bf16[1024,512]{1,0:T(8,128)(2,1)} custom-call(bf16[1024,512]{1,0:T(8,128)(2,1)} %bitcast.9, bf16[1024,128]{1,0:T(8,128)(2,1)} %keys1_ref.1, bf16[1024,128]{1,0:T(8,128)(2,1)} %queries1_ref.1, bf16[64,1024]{1,0:T(8,128)(2,1)} %bitcast.13, bf16[64,1024]{1,0:T(8,128)(2,1)} %bitcast.14, f32[2,4,1024]{2,1,0:T(4,128)} %bitcast.15, ...), custom_call_target="tpu_custom_call" | custom-call | tf_op jit(solution)/shard_map/layer/pallas_call | solution.py:820
  204.6 2.3 %copy.23 = bf16[1024,512]{1,0:T(8,128)(2,1)} copy(bf16[1024,512]{1,0:T(8,128)(2,1)} %layer.1) | data formatting | bytes 2097152
Async XLA Ops:
  0.0 2.5 %copy-start = (bf16[1024,2,256]{2,1,0:T(2,128)(2,1)S(1)}, bf16[1024,2,256]{2,1,0:T(2,128)(2,1)}, u32[]{:S(2)}) copy-start(bf16[1024,2,256]{2,1,0:T(2,128)(2,1)} %param.20) | copy-start | bytes 3145732

commit v2 on v1

--- a/solution.py
+++ b/solution.py
@@ -39,7 +39,7 @@
     head_taps_ref, taps1_ref, taps2_ref, hgain_ref, cgain_ref,
     gate_in, wout_in, res_in, wg_ref, wu_ref, wd_ref,
     out_ref,
-    gate_ref, wout_ref, res_ref, in_sems, taps_ref, step_rows, log_rows, rim_out, xs, rim, vals, kq, cums, st, stsend, strecv, mix, stream, normed, weights, hidden,
+    gate_ref, wout_ref, res_ref, in_sems, taps_ref, step_rows, log_rows, rim_out, xs, rim, vals, kq, cums, st, stsend, entering, strecv, mix, stream, normed, weights, hidden,
     give, give_recv, sums, across_recv, ready, sums_recv,
     rim_sems, st_send, st_recv, m_send, m_fwd, m_recv, r_send, r_fwd, r_recv,
     p_send, p_fwd, p_recv, w_local, w_pair, w_send, w_recv,
@@ -104,8 +104,13 @@
         along(w, s, True).wait_recv()
 
     def start_weights():
+        give_pair(0).start()
+
+        @pl.when(y == 1)
+        def _():
+            give_pair(1).start()
+
         for w in range(2):
-            give_pair(w).start()
             send_along(w, me, False, own=True)
         send_along(0, me, True, own=True)
         for w in range(3):
@@ -176,12 +181,12 @@
         device_id_type=MESH,
     )
 
-    start_weights()
-
     @pl.when(me < n - 1)
     def _():
         rim_out[...] = tokens_of(nb - 1)[BLOCK - RIM :].astype(jnp.bfloat16)
         rim_copy.start()
+
+    start_weights()
 
     for copy in later:
         copy.start()
@@ -280,18 +285,18 @@
             for g in range(2)
         ]
 
-    def state_copy(to, source):
+    def state_copy(to, source, packed):
         return pltpu.make_async_remote_copy(
-            src_ref=stsend,
-            dst_ref=strecv.at[source],
+            src_ref=packed,
+            dst_ref=strecv.at[source, pl.ds(0, packed.shape[0])],
             send_sem=st_send.at[to],
             recv_sem=st_recv.at[source],
             device_id={"sp": to},
             device_id_type=MESH,
         )
 
-    def send_state(to, carry):
-        state_copy(to, me).start()
+    def send_state(i, carry):
+        state_copy(n - 1 - 2 * i, me, stsend).start()
         return carry
 
     own_logs = [spread(total, g * heads, heads) for g in range(2)]
@@ -299,11 +304,13 @@
     @pl.when(y == 0)
     def _():
         pack_state(own_logs)
-        state_copy(pair, me).start()
+        state_copy(pair, me, stsend).start()
+        give_pair(1).start()
+        give_pair(2).start()
 
     @pl.when(y == 1)
     def _():
-        state_copy(me, pair).wait_recv()
+        state_copy(me, pair, stsend).wait_recv()
         got = strecv[pair].astype(jnp.float32)
         for g in range(2):
             base, size = (0, s1) if g == 0 else (s1, s2)
@@ -312,13 +319,20 @@
             )
         both = [a + b for a, b in zip(logs_of(got), own_logs)]
         pack_state(both)
-        lax.fori_loop(me + 1, n, send_state, 0)
-
-    send_along(1, me, True, own=True)
-    for w in range(2):
+        lax.fori_loop(0, m - 1 - q, send_state, 0)
+
+    def relay_pair(w):
         take_unit(w, pair)
         send_along(w, pair, False)
         send_along(w, pair, True)
+
+    send_along(1, me, True, own=True)
+    relay_pair(0)
+
+    @pl.when(y == 0)
+    def _():
+        relay_pair(1)
+
     st[...] = jnp.zeros_like(st)
 
     def add_state(source):
@@ -332,15 +346,27 @@
 
     def take_state(before, carry):
         source = before * 2 + 1
-        state_copy(n - 1, source).wait_recv()
+        state_copy(n - 1, source, stsend).wait_recv()
         add_state(source)
         return carry
-
-    lax.fori_loop(0, q, take_state, 0)
 
     @pl.when(y == 1)
     def _():
+        lax.fori_loop(0, q, take_state, 0)
+
+        @pl.when(q > 0)
+        def _():
+            entering[...] = st[...].astype(jnp.bfloat16)
+            state_copy(pair, me, entering).start()
+
+        give_pair(2).start()
         add_state(pair)
+        relay_pair(1)
+
+    @pl.when((y == 0) & (q > 0))
+    def _():
+        state_copy(me, pair, entering).wait_recv()
+        st[...] = strecv[pair, 0:states].astype(jnp.float32)
 
     def share(buf, yy, source, b, sp, to, send, recv):
         piece = buf.at[yy, source, rows_of(b)]
@@ -473,10 +499,6 @@
         def _():
             project(b - 2)
 
-        @pl.when(b == nb)
-        def _():
-            give_pair(2).start()
-
         @pl.when(b == nb + 3)
         def _():
             send_along(down, me, False, own=True)
@@ -544,22 +566,9 @@
     tall = 2 * BLOCK
     pieces = tokens // tall
 
-    def mix_channels(i, carry):
-        yy = i // pieces
-        r = pl.ds(pl.multiple_of(lax.rem(i, pieces) * tall, tall), tall)
-        rows = normed[yy, r]
-        g = jnp.dot(rows, weights[0], preferred_element_type=jnp.float32)
-        u = jnp.dot(rows, weights[1], preferred_element_type=jnp.float32)
-        hidden[yy, r] = (g * sigmoid(g) * u).astype(jnp.bfloat16)
-        return carry
-
-    lax.fori_loop(0, 2 * pieces, mix_channels, 0)
-
     def pass_on(d, carry):
         relay_far(d)
         return carry
-
-    lax.fori_loop(2, m, pass_on, 0)
 
     near = jnp.minimum(q, m - 1 - q)
 
@@ -627,36 +636,41 @@
 
     keeps = core == y
 
+    def give_piece(i, p):
+        k = chunk_at(i)
+
+        @pl.when(i >= 2)
+        def _():
+            give_copy(i, k, p).wait_send()
+
+        give[lax.rem(i, 2), rows_at(p)] = product(1 - core, k, p).astype(jnp.bfloat16)
+        give_copy(i, k, p).start()
+
+    def sum_piece(i, p):
+        k = chunk_at(i)
+
+        @pl.when(jnp.logical_not(keeps) & (i >= 2))
+        def _():
+            pair_copy(i, k, p).wait_send()
+
+        give_copy(i, k, p).wait_recv()
+        both = product(core, k, p) + give_recv[k, rows_at(p)].astype(jnp.float32)
+        sums[lax.rem(i, 2), rows_at(p)] = both.astype(jnp.bfloat16)
+
+        @pl.when(jnp.logical_not(keeps))
+        def _():
+            pair_copy(i, k, p).start()
+
     def give_half(i):
-        k = chunk_at(i)
-
         def one(p, carry):
-            @pl.when(i >= 2)
-            def _():
-                give_copy(i, k, p).wait_send()
-
-            give[lax.rem(i, 2), rows_at(p)] = product(1 - core, k, p).astype(jnp.bfloat16)
-            give_copy(i, k, p).start()
+            give_piece(i, p)
             return carry
 
         lax.fori_loop(0, pieces, one, 0)
 
     def sum_half(i):
-        k = chunk_at(i)
-
         def one(p, carry):
-            @pl.when(jnp.logical_not(keeps) & (i >= 2))
-            def _():
-                pair_copy(i, k, p).wait_send()
-
-            give_copy(i, k, p).wait_recv()
-            both = product(core, k, p) + give_recv[k, rows_at(p)].astype(jnp.float32)
-            sums[lax.rem(i, 2), rows_at(p)] = both.astype(jnp.bfloat16)
-
-            @pl.when(jnp.logical_not(keeps))
-            def _():
-                pair_copy(i, k, p).start()
-
+            sum_piece(i, p)
             return carry
 
         lax.fori_loop(0, pieces, one, 0)
@@ -691,32 +705,82 @@
 
         lax.fori_loop(0, pieces, one, 0)
 
+    def take_all(i, carry):
+        take_down(i)
+        return carry
+
+    def first_part(i):
+        @pl.when(keeps)
+        def _():
+            give_half(i)
+
+        @pl.when(jnp.logical_not(keeps))
+        def _():
+            sum_half(i)
+
+    def second_part(i):
+        @pl.when(keeps)
+        def _():
+            sum_half(i)
+
+        @pl.when(jnp.logical_not(keeps))
+        def _():
+            give_half(i)
+
     if units > 1:
-
-        def take_all(i, carry):
-            take_down(i)
-            return carry
-
+        lax.fori_loop(2, m, pass_on, 0)
         lax.fori_loop(0, n, take_all, 0)
 
+    def mix_channels(yy, p):
+        rows = normed[yy, rows_at(p)]
+        g = jnp.dot(rows, weights[0], preferred_element_type=jnp.float32)
+        u = jnp.dot(rows, weights[1], preferred_element_type=jnp.float32)
+        hidden[yy, rows_at(p)] = (g * sigmoid(g) * u).astype(jnp.bfloat16)
+
+    ahead = min(2, chunks)
+
+    def mix_step(j, carry):
+        p = lax.rem(j, pieces)
+        theirs = j < pieces
+        mix_channels(jnp.where(theirs, 1 - y, y), p)
+
+        @pl.when(theirs & keeps)
+        def _():
+            give_piece(0, p)
+
+        @pl.when(theirs & jnp.logical_not(keeps))
+        def _():
+            sum_piece(0, p)
+
+        @pl.when(j == pieces - 1)
+        def _():
+            if ahead > 1:
+                first_part(1)
+
+        return carry
+
+    lax.fori_loop(0, 2 * pieces, mix_step, 0)
+    if units == 1:
+        lax.fori_loop(2, m, pass_on, 0)
+
     def chunk_step(i, carry):
-        @pl.when(i < chunks)
+        @pl.when((i >= ahead) & (i < chunks))
         def _():
             if units == 1:
                 take_down(i)
-            give_half(i)
-
-        @pl.when((i >= 1) & (i < chunks + 1))
-        def _():
-            sum_half(i - 1)
-
-        @pl.when(keeps & (i >= 2))
-        def _():
-            sum_pair(i - 2)
-
-        return carry
-
-    lax.fori_loop(0, chunks + 2, chunk_step, 0)
+            first_part(i)
+
+        @pl.when(i < chunks)
+        def _():
+            second_part(i)
+
+        @pl.when(keeps & (i >= 1))
+        def _():
+            sum_pair(i - 1)
+
+        return carry
+
+    lax.fori_loop(0, chunks + 1, chunk_step, 0)
 
     def finish(p, carry):
         r = rows_at(p)
@@ -758,11 +822,21 @@
     def _():
         rim_copy.wait_send()
 
-    def end_state(to, carry):
-        state_copy(to, me).wait_send()
-        return carry
-
-    lax.fori_loop(me + 1, jnp.where(y == 0, me + 2, n), end_state, 0)
+    def end_state(i, carry):
+        state_copy(n - 1 - 2 * i, me, stsend).wait_send()
+        return carry
+
+    @pl.when(y == 0)
+    def _():
+        state_copy(pair, me, stsend).wait_send()
+
+    @pl.when(y == 1)
+    def _():
+        lax.fori_loop(0, m - 1 - q, end_state, 0)
+
+        @pl.when(q > 0)
+        def _():
+            state_copy(pair, me, entering).wait_send()
 
     def end_shares(b, carry):
         for buf, yy, send, fwd, recv in (
@@ -841,6 +915,7 @@
             pltpu.VMEM((tokens, BLOCK), jnp.float32),
             pltpu.VMEM((s1 + s2, half), jnp.float32),
             pltpu.VMEM((s1 + s2 + RIM, half), jnp.bfloat16),
+            pltpu.VMEM((s1 + s2, half), jnp.bfloat16),
             pltpu.VMEM((n, s1 + s2 + RIM, half), jnp.bfloat16),
             pltpu.VMEM((1, tp, tokens, 2 * half), jnp.bfloat16),
             pltpu.VMEM((2, tp, tokens, cols), jnp.bfloat16),

time: 207 us -> 187 us (0.903)
  the two profiles are of different devices: /device:TPU:24 before, /device:TPU:28 now
where the time goes in v2:
time: 187 us
  Pallas kernels  181 us (97%)
  local copies, waits for them, and re-layouts  5.99 us (3%)
    pallas_call x1, Pallas kernels, layer(): pl.pallas_call(functools.partial(layer_kernel, n, tp, heads, s1, s2, spli...  181 us
    unnamed x5, local copies, waits for them, and re-layouts  5.99 us

profile of v2, /device:TPU:28, one launch (start us, length us, event | category | flops | bytes accessed | tf_op | source)
XLA Modules:
  0.0 186.9 jit_solution(11022643955424840179)
XLA Ops:
  0.0 0.0 copy-start
  0.0 2.5 %copy.20 = bf16[128,8,2,256]{3,1,2,0:T(8,128)(2,1)} copy(bf16[128,8,2,256]{3,2,1,0:T(2,128)(2,1)} %bitcast.11) | data formatting | bytes 2097152
  2.5 0.0 copy-done
  2.5 1.2 copy.21
  3.7 180.9 %layer.1 = bf16[1024,512]{1,0:T(8,128)(2,1)} custom-call(bf16[1024,512]{1,0:T(8,128)(2,1)} %bitcast.9, bf16[1024,128]{1,0:T(8,128)(2,1)} %keys1_ref.1, bf16[1024,128]{1,0:T(8,128)(2,1)} %queries1_ref.1, bf16[64,1024]{1,0:T(8,128)(2,1)} %bitcast.13, bf16[64,1024]{1,0:T(8,128)(2,1)} %bitcast.14, f32[2,4,1024]{2,1,0:T(4,128)} %bitcast.15, ...), custom_call_target="tpu_custom_call" | custom-call | tf_op jit(solution)/shard_map/layer/pallas_call | solution.py:894
  184.6 2.3 %copy.23 = bf16[1024,512]{1,0:T(8,128)(2,1)} copy(bf16[1024,512]{1,0:T(8,128)(2,1)} %layer.1) | data formatting | bytes 2097152
Async XLA Ops:
  0.0 2.5 %copy-start = (bf16[1024,2,256]{2,1,0:T(2,128)(2,1)S(1)}, bf16[1024,2,256]{2,1,0:T(2,128)(2,1)}, u32[]{:S(2)}) copy-start(bf16[1024,2,256]{2,1,0:T(2,128)(2,1)} %param.20) | copy-start | bytes 3145732

commit v3 on v2

--- a/solution.py
+++ b/solution.py
@@ -13,6 +13,7 @@
 RIM = 16
 EPSILON = 1e-06
 LANES = 128
+SLOTS = 4
 VMEM_LIMIT = 63 << 20
 MESH = pl.DeviceIdType.MESH
 
@@ -112,7 +113,7 @@
 
         for w in range(2):
             send_along(w, me, False, own=True)
-        send_along(0, me, True, own=True)
+            send_along(w, me, True, own=True)
         for w in range(3):
             keep_own(w).start()
 
@@ -137,20 +138,22 @@
     early = 4 * (m - 1)
     stride = max(m - 3, 0)
 
-    def relay_points(b, first, go):
-        for j, at in enumerate((0, 1, 3, 4)):
-
-            @pl.when(b == first + at)
+    def relay_points(b):
+        for j, at in ((6, 1), (7, 3)):
+
+            @pl.when(b == at)
             def _():
                 if m > 2:
-                    go(4 + j)
+                    relay_down(j)
+                    relay_up(j)
 
         for j in range(4):
 
-            @pl.when(b == first + nb - 2 + j)
+            @pl.when(b == nb - 3 + j)
             def _():
                 for i in range(stride):
-                    go(8 + j * stride + i)
+                    relay_down(8 + j * stride + i)
+                    relay_up(8 + j * stride + i)
 
     later = [
         pltpu.make_async_copy(source, place, in_sems.at[i])
@@ -326,7 +329,6 @@
         send_along(w, pair, False)
         send_along(w, pair, True)
 
-    send_along(1, me, True, own=True)
     relay_pair(0)
 
     @pl.when(y == 0)
@@ -488,8 +490,7 @@
         def _():
             second_pass(b)
 
-        relay_points(b, 0, relay_down)
-        relay_points(b, 1, relay_up)
+        relay_points(b)
 
         @pl.when((b >= 1) & (b < nb + 1))
         def _():
@@ -499,10 +500,16 @@
         def _():
             project(b - 2)
 
-        @pl.when(b == nb + 3)
-        def _():
-            send_along(down, me, False, own=True)
-            send_along(down, me, True, own=True)
+        for turn in range(2):
+
+            @pl.when((b == nb + 1 + turn) & (y == turn))
+            def _():
+                send_along(down, me, False, own=True)
+                send_along(down, me, True, own=True)
+
+            @pl.when((b == nb + 1 + turn) & (y != turn))
+            def _():
+                relay_pair(down)
 
         @pl.when((b >= 3) & (b < nb + 3))
         def _():
@@ -529,8 +536,13 @@
 
     for copy in later:
         copy.wait()
+    if m > 2:
+        for k in (4, 5):
+            relay_down(k)
+            relay_up(k)
     lax.fori_loop(0, nb + 7, stage, 0)
 
+    units = sums.shape[2] // shard
     between = (q > 0) & (q < m - 1)
 
     def relay_far(d):
@@ -549,10 +561,8 @@
                 send_along(down, s, True)
 
     keep_own(down).wait()
-    take_unit(down, pair)
-    send_along(down, pair, False)
-    send_along(down, pair, True)
-    relay_far(1)
+    if units > 1:
+        relay_far(1)
 
     def late(k, carry):
         relay_down(k)
@@ -579,7 +589,6 @@
         return jnp.where(i <= 2 * near, side, beyond)
 
     width = sums.shape[2]
-    units = width // shard
     chunks = tp * cols // width
     per_owner = cols // width
 
@@ -594,8 +603,8 @@
     def chunk_at(i):
         return shard_at(i) if units == 1 else i
 
-    def product(yy, k, p):
-        r = pl.ds(pl.multiple_of(p * tall, tall), tall)
+    def product(yy, k, p, count):
+        r = pl.ds(pl.multiple_of(p * tall, tall), count * tall)
         block = weights[down, pl.ds(pl.multiple_of(k * width, width), width)]
         return lax.dot_general(
             hidden[yy, r], block, (((1,), (1,)), ((), ())), preferred_element_type=jnp.float32
@@ -616,9 +625,9 @@
 
     def pair_copy(i, k, p):
         return pltpu.make_async_remote_copy(
-            src_ref=sums.at[lax.rem(i, 2), rows_at(p)],
+            src_ref=sums.at[lax.rem(i, slots), rows_at(p)],
             dst_ref=across_recv.at[k, rows_at(p)],
-            send_sem=a_send.at[lax.rem(i, 2), p],
+            send_sem=a_send.at[lax.rem(i, slots), p],
             recv_sem=a_recv.at[k, p],
             device_id={"sp": pair},
             device_id_type=MESH,
@@ -626,75 +635,84 @@
 
     def owner_copy(i, k, p, source):
         return pltpu.make_async_remote_copy(
-            src_ref=ready.at[lax.rem(i, 2), rows_at(p)],
+            src_ref=ready.at[lax.rem(i, slots), rows_at(p)],
             dst_ref=sums_recv.at[source, lax.rem(k, per_owner), rows_at(p)],
-            send_sem=s_send.at[lax.rem(i, 2), p],
+            send_sem=s_send.at[lax.rem(i, slots), p],
             recv_sem=s_recv.at[source, lax.rem(k, per_owner), p],
             device_id={"tp": k // per_owner},
             device_id_type=MESH,
         )
 
     keeps = core == y
-
-    def give_piece(i, p):
+    slots = sums.shape[0]
+
+    def give_piece(i, p, count=1):
         k = chunk_at(i)
-
-        @pl.when(i >= 2)
-        def _():
-            give_copy(i, k, p).wait_send()
-
-        give[lax.rem(i, 2), rows_at(p)] = product(1 - core, k, p).astype(jnp.bfloat16)
-        give_copy(i, k, p).start()
-
-    def sum_piece(i, p):
+        for c in range(count):
+
+            @pl.when(i >= 2)
+            def _():
+                give_copy(i, k, p + c).wait_send()
+
+        r = pl.ds(pl.multiple_of(p * tall, tall), count * tall)
+        give[lax.rem(i, 2), r] = product(1 - core, k, p, count).astype(jnp.bfloat16)
+        for c in range(count):
+            give_copy(i, k, p + c).start()
+
+    def sum_piece(i, p, count=1):
         k = chunk_at(i)
-
-        @pl.when(jnp.logical_not(keeps) & (i >= 2))
-        def _():
-            pair_copy(i, k, p).wait_send()
-
-        give_copy(i, k, p).wait_recv()
-        both = product(core, k, p) + give_recv[k, rows_at(p)].astype(jnp.float32)
-        sums[lax.rem(i, 2), rows_at(p)] = both.astype(jnp.bfloat16)
+        for c in range(count):
+
+            @pl.when(jnp.logical_not(keeps) & (i >= slots))
+            def _():
+                pair_copy(i, k, p + c).wait_send()
+
+            give_copy(i, k, p + c).wait_recv()
+        r = pl.ds(pl.multiple_of(p * tall, tall), count * tall)
+        both = product(core, k, p, count) + give_recv[k, r].astype(jnp.float32)
+        sums[lax.rem(i, slots), r] = both.astype(jnp.bfloat16)
 
         @pl.when(jnp.logical_not(keeps))
         def _():
-            pair_copy(i, k, p).start()
+            for c in range(count):
+                pair_copy(i, k, p + c).start()
+
+    many = 2 if pieces % 2 == 0 else 1
 
     def give_half(i):
         def one(p, carry):
-            give_piece(i, p)
+            give_piece(i, p * many, many)
             return carry
 
-        lax.fori_loop(0, pieces, one, 0)
+        lax.fori_loop(0, pieces // many, one, 0)
 
     def sum_half(i):
         def one(p, carry):
-            sum_piece(i, p)
+            sum_piece(i, p * many, many)
             return carry
 
-        lax.fori_loop(0, pieces, one, 0)
+        lax.fori_loop(0, pieces // many, one, 0)
 
     def sum_pair(i):
         k = chunk_at(i)
         away = k // per_owner != t
-        before = chunk_at(jnp.maximum(i - 2, 0))
+        before = chunk_at(jnp.maximum(i - slots, 0))
 
         def one(p, carry):
-            @pl.when((i >= 2) & (before // per_owner != t))
+            @pl.when((i >= slots) & (before // per_owner != t))
             def _():
                 owner_copy(i, before, p, my_x).wait_send()
 
             pair_copy(i, k, p).wait_recv()
             r = rows_at(p)
-            both = sums[lax.rem(i, 2), r].astype(jnp.float32) + across_recv[k, r].astype(
+            both = sums[lax.rem(i, slots), r].astype(jnp.float32) + across_recv[k, r].astype(
                 jnp.float32
             )
             both = both.astype(jnp.bfloat16)
 
             @pl.when(away)
             def _():
-                ready[lax.rem(i, 2), r] = both
+                ready[lax.rem(i, slots), r] = both
                 owner_copy(i, k, p, my_x).start()
 
             @pl.when(jnp.logical_not(away))
@@ -708,24 +726,6 @@
     def take_all(i, carry):
         take_down(i)
         return carry
-
-    def first_part(i):
-        @pl.when(keeps)
-        def _():
-            give_half(i)
-
-        @pl.when(jnp.logical_not(keeps))
-        def _():
-            sum_half(i)
-
-    def second_part(i):
-        @pl.when(keeps)
-        def _():
-            sum_half(i)
-
-        @pl.when(jnp.logical_not(keeps))
-        def _():
-            give_half(i)
 
     if units > 1:
         lax.fori_loop(2, m, pass_on, 0)
@@ -739,6 +739,18 @@
 
     ahead = min(2, chunks)
 
+    def pair_half(i):
+        if units == 1:
+            take_down(i)
+
+        @pl.when(keeps)
+        def _():
+            give_half(i)
+
+        @pl.when(jnp.logical_not(keeps))
+        def _():
+            sum_half(i)
+
     def mix_step(j, carry):
         p = lax.rem(j, pieces)
         theirs = j < pieces
@@ -746,41 +758,86 @@
 
         @pl.when(theirs & keeps)
         def _():
-            give_piece(0, p)
+            for i in range(ahead):
+                give_piece(i, p)
 
         @pl.when(theirs & jnp.logical_not(keeps))
         def _():
-            sum_piece(0, p)
+            for i in range(ahead):
+                sum_piece(i, p)
 
         @pl.when(j == pieces - 1)
         def _():
-            if ahead > 1:
-                first_part(1)
+            if units == 1:
+                relay_far(1)
+            if chunks > ahead:
+                pair_half(ahead)
+
+        @pl.when(j == 2 * pieces - 2)
+        def _():
+            if chunks > ahead + 1:
+                pair_half(ahead + 1)
 
         return carry
 
     lax.fori_loop(0, 2 * pieces, mix_step, 0)
-    if units == 1:
-        lax.fori_loop(2, m, pass_on, 0)
+
+    middle = chunks // 2
 
     def chunk_step(i, carry):
-        @pl.when((i >= ahead) & (i < chunks))
-        def _():
-            if units == 1:
-                take_down(i)
-            first_part(i)
-
-        @pl.when(i < chunks)
-        def _():
-            second_part(i)
-
-        @pl.when(keeps & (i >= 1))
-        def _():
-            sum_pair(i - 1)
-
-        return carry
-
-    lax.fori_loop(0, chunks + 1, chunk_step, 0)
+        early = (i >= 1) & (i < middle - 1)
+        late_on = (i > middle) & (i < chunks - 1)
+        far = jnp.where(i < middle, i + 3, i + 1)
+
+        if units == 1:
+
+            @pl.when(i == min(2, chunks - 1))
+            def _():
+                lax.fori_loop(2, m, pass_on, 0)
+
+        @pl.when(jnp.logical_not(keeps))
+        def _():
+            give_half(i)
+
+        if units == 1:
+
+            @pl.when(early)
+            def _():
+                take_down(far)
+
+        @pl.when(keeps & early)
+        def _():
+            give_half(far)
+
+        @pl.when(keeps)
+        def _():
+            sum_half(i)
+
+            @pl.when(i >= 1)
+            def _():
+                sum_pair(i - 1)
+
+        if units == 1:
+
+            @pl.when(late_on)
+            def _():
+                take_down(far)
+
+        @pl.when(keeps & late_on)
+        def _():
+            give_half(far)
+
+        @pl.when(jnp.logical_not(keeps) & (early | late_on))
+        def _():
+            sum_half(far)
+
+        return carry
+
+    lax.fori_loop(0, chunks, chunk_step, 0)
+
+    @pl.when(keeps)
+    def _():
+        sum_pair(chunks - 1)
 
     def finish(p, carry):
         r = rows_at(p)
@@ -803,8 +860,9 @@
 
     def end_sums(p, carry):
         for i in range(max(chunks - 2, 0), chunks):
+            give_copy(i, chunk_at(i), p).wait_send()
+        for i in range(max(chunks - slots, 0), chunks):
             last = chunk_at(i)
-            give_copy(i, last, p).wait_send()
 
             @pl.when(jnp.logical_not(keeps))
             def _():
@@ -924,21 +982,21 @@
             pltpu.VMEM((2, tokens, part), jnp.bfloat16),
             pltpu.VMEM((2, tokens, width), jnp.bfloat16),
             pltpu.VMEM((chunks, tokens, width), jnp.bfloat16),
-            pltpu.VMEM((2, tokens, width), jnp.bfloat16),
+            pltpu.VMEM((SLOTS, tokens, width), jnp.bfloat16),
             pltpu.VMEM((chunks, tokens, width), jnp.bfloat16),
-            pltpu.VMEM((2, tokens, width), jnp.bfloat16),
+            pltpu.VMEM((SLOTS, tokens, width), jnp.bfloat16),
             pltpu.VMEM((tp // 2, cols // width, tokens, width), jnp.bfloat16),
             dma((2,)),
             dma((n,)),
             dma((n,)),
+            dma((tp // 2, nb)),
+            dma((tp // 2, nb)),
             dma((tp, nb)),
+            dma((tp // 2, nb)),
+            dma((tp // 2, nb)),
             dma((tp, nb)),
-            dma((tp, nb)),
-            dma((tp, nb)),
-            dma((tp, nb)),
-            dma((tp, nb)),
-            dma((tp, nb)),
-            dma((tp, nb)),
+            dma((tp // 2, nb)),
+            dma((tp // 2, nb)),
             dma((tp, nb)),
             dma((3,)),
             dma((3,)),
@@ -946,9 +1004,9 @@
             dma((3, n)),
             dma((2, pieces)),
             dma((chunks, pieces)),
-            dma((2, pieces)),
+            dma((SLOTS, pieces)),
             dma((chunks, pieces)),
-            dma((2, pieces)),
+            dma((SLOTS, pieces)),
             dma((tp // 2, cols // width, pieces)),
         ],
         compiler_params=pltpu.CompilerParams(

time: 187 us -> 172 us (0.920)
  Pallas kernels: 181 us -> 166 us
    pallas_call x1, Pallas kernels: 181 us -> 166 us  [layer(): pl.pallas_call(functools.partial(layer_kernel, n, tp, heads, s1, s2, spli...]
where the time goes in v3:
time: 172 us
  Pallas kernels  166 us (97%)
  local copies, waits for them, and re-layouts  5.99 us (3%)
    pallas_call x1, Pallas kernels, layer(): pl.pallas_call(functools.partial(layer_kernel, n, tp, heads, s1, s2, spli...  166 us
    unnamed x5, local copies, waits for them, and re-layouts  5.99 us

profile of v3, /device:TPU:28, one launch (start us, length us, event | category | flops | bytes accessed | tf_op | source)
XLA Modules:
  0.0 172.3 jit_solution(14108541839456213979)
XLA Ops:
  0.0 0.0 copy-start
  0.0 2.5 %copy.20 = bf16[128,8,2,256]{3,1,2,0:T(8,128)(2,1)} copy(bf16[128,8,2,256]{3,2,1,0:T(2,128)(2,1)} %bitcast.11) | data formatting | bytes 2097152
  2.5 0.0 copy-done
  2.5 1.2 copy.21
  3.7 166.3 %layer.1 = bf16[1024,512]{1,0:T(8,128)(2,1)} custom-call(bf16[1024,512]{1,0:T(8,128)(2,1)} %bitcast.9, bf16[1024,128]{1,0:T(8,128)(2,1)} %keys1_ref.1, bf16[1024,128]{1,0:T(8,128)(2,1)} %queries1_ref.1, bf16[64,1024]{1,0:T(8,128)(2,1)} %bitcast.13, bf16[64,1024]{1,0:T(8,128)(2,1)} %bitcast.14, f32[2,4,1024]{2,1,0:T(4,128)} %bitcast.15, ...), custom_call_target="tpu_custom_call" | custom-call | tf_op jit(solution)/shard_map/layer/pallas_call | solution.py:952
  170.0 2.3 %copy.23 = bf16[1024,512]{1,0:T(8,128)(2,1)} copy(bf16[1024,512]{1,0:T(8,128)(2,1)} %layer.1) | data formatting | bytes 2097152
Async XLA Ops:
  0.0 2.5 %copy-start = (bf16[1024,2,256]{2,1,0:T(2,128)(2,1)S(1)}, bf16[1024,2,256]{2,1,0:T(2,128)(2,1)}, u32[]{:S(2)}) copy-start(bf16[1024,2,256]{2,1,0:T(2,128)(2,1)} %param.20) | copy-start | bytes 3145732

commit v4 on v3

--- a/solution.py
+++ b/solution.py
@@ -165,9 +165,11 @@
     def tokens_of(b):
         r = rows_of(b)
         second = jnp.concatenate([keys2_ref[:, r], queries2_ref[:, r]], axis=0)
+        heads_in = x_ref[r].astype(jnp.float32)
         return jnp.concatenate(
             [
-                x_ref[r].astype(jnp.float32),
+                heads_in[:, 0, :],
+                heads_in[:, 1, :],
                 keys1_ref[r].astype(jnp.float32),
                 queries1_ref[r].astype(jnp.float32),
                 second.astype(jnp.float32).T,
@@ -423,6 +425,8 @@
         cum = cums[r]
         cum_t = cum.T
         grown = jnp.exp(cum)
+        both = gate_ref[r].astype(jnp.float32)
+        gates = [both[:, g, :] for g in range(2)]
         for g in range(2):
             off, size = (0, s1) if g == 0 else (2 * s1, s2)
             base = 0 if g == 0 else s1
@@ -446,7 +450,7 @@
                 lanes = slice(h * HEAD, (h + 1) * HEAD)
                 y = jnp.dot(w, v[:, lanes], preferred_element_type=jnp.float32)
                 y = y + carried[:, lanes]
-                z = gate_ref[r, g * half + h * HEAD : g * half + (h + 1) * HEAD].astype(jnp.float32)
+                z = gates[g][:, lanes]
                 y = y * (z * sigmoid(z))
                 y = y * lax.rsqrt(jnp.mean(y * y, axis=1, keepdims=True) + EPSILON)
                 outs.append(y)
@@ -809,13 +813,17 @@
         def _():
             give_half(far)
 
+        @pl.when(keeps & (i >= chunks - 2) & (i >= 1))
+        def _():
+            sum_pair(i - 1)
+
         @pl.when(keeps)
         def _():
             sum_half(i)
 
-            @pl.when(i >= 1)
-            def _():
-                sum_pair(i - 1)
+        @pl.when(keeps & (i < chunks - 2) & (i >= 1))
+        def _():
+            sum_pair(i - 1)
 
         if units == 1:
 
@@ -1037,13 +1045,11 @@
     channel_up_weight,
     channel_down_weight,
 ):
-    tokens = grouped_head_inputs.shape[0]
     heads = head_decay_rate.shape[1]
-    half = heads * HEAD
     s1, s2 = first_group_keys.shape[1], second_group_keys.shape[1]
     return layer(
         (
-            grouped_head_inputs.reshape(tokens, 2 * half),
+            grouped_head_inputs,
             first_group_keys,
             first_group_queries,
             second_group_keys.T,
@@ -1057,7 +1063,7 @@
             head_norm_gain,
             channel_norm_gain.reshape(1, -1),
         ),
-        (head_gate_inputs.reshape(tokens, 2 * half), output_weight, residual),
+        (head_gate_inputs, output_weight, residual),
         channel_gate_weight,
         channel_up_weight,
         channel_down_weight,

time: 172 us -> 168 us (0.977)
  local copies, waits for them, and re-layouts: 5.99 us -> 2.26 us
    unnamed x5 -> x1, local copies, waits for them, and re-layouts: 5.99 us -> 2.26 us
where the time goes in v4:
time: 168 us
  Pallas kernels  166 us (99%)
  local copies, waits for them, and re-layouts  2.26 us (1%)
    pallas_call x1, Pallas kernels, layer(): pl.pallas_call(functools.partial(layer_kernel, n, tp, heads, s1, s2, spli...  166 us

profile of v4, /device:TPU:28, one launch (start us, length us, event | category | flops | bytes accessed | tf_op | source)
XLA Modules:
  0.0 168.2 jit_solution(5975276258368981556)
XLA Ops:
  0.0 165.9 %layer.1 = bf16[1024,512]{1,0:T(8,128)(2,1)} custom-call(bf16[1024,2,256]{2,1,0:T(2,128)(2,1)} %x_ref.1, bf16[1024,128]{1,0:T(8,128)(2,1)} %keys1_ref.1, bf16[1024,128]{1,0:T(8,128)(2,1)} %queries1_ref.1, bf16[64,1024]{1,0:T(8,128)(2,1)} %bitcast.5, bf16[64,1024]{1,0:T(8,128)(2,1)} %bitcast.6, f32[2,4,1024]{2,1,0:T(4,128)} %bitcast.7, ...), custom_call_target="tpu_custom_call" | custom-call | tf_op jit(solution)/shard_map/layer/pallas_call | solution.py:960
  165.9 2.3 %copy.21 = bf16[1024,512]{1,0:T(8,128)(2,1)} copy(bf16[1024,512]{1,0:T(8,128)(2,1)} %layer.1) | data formatting | bytes 2097152

commit v5 on v4

--- a/solution.py
+++ b/solution.py
@@ -111,9 +111,11 @@
         def _():
             give_pair(1).start()
 
-        for w in range(2):
-            send_along(w, me, False, own=True)
-            send_along(w, me, True, own=True)
+        @pl.when(y == 1)
+        def _():
+            for w in range(2):
+                send_along(w, me, True, own=True)
+
         for w in range(3):
             keep_own(w).start()
 
@@ -185,6 +187,14 @@
         device_id={"sp": lax.rem(me + 1, n)},
         device_id_type=MESH,
     )
+
+    for w in range(2):
+        send_along(w, me, False, own=True)
+
+    @pl.when(y == 0)
+    def _():
+        for w in range(2):
+            send_along(w, me, True, own=True)
 
     @pl.when(me < n - 1)
     def _():
@@ -395,7 +405,7 @@
     def forward(buf, yy, b, fwd, recv):
         for d in range(1, nx):
             source = across(d) + core
-            move = share(buf, yy, source, b, me, partner, fwd.at[d, b], recv)
+            move = share(buf, yy, source, b, me, partner, fwd.at[d - 1, b], recv)
             move.wait_recv()
             move.start()
 
@@ -912,7 +922,7 @@
             for d in range(nx):
                 share(buf, yy, t, b, me, partner, send.at[d, b], recv).wait_send()
             for d in range(1, nx):
-                share(buf, yy, t, b, me, partner, fwd.at[d, b], recv).wait_send()
+                share(buf, yy, t, b, me, partner, fwd.at[d - 1, b], recv).wait_send()
         for d in range(nx):
             share(stream, y, t, b, me, partner, p_send.at[d, b], p_recv).wait_send()
             share(stream, y, t, b, me, partner, p_fwd.at[d, b], p_recv).wait_send()
@@ -998,10 +1008,10 @@
             dma((n,)),
             dma((n,)),
             dma((tp // 2, nb)),
-            dma((tp // 2, nb)),
+            dma((max(tp // 2 - 1, 1), nb)),
             dma((tp, nb)),
             dma((tp // 2, nb)),
-            dma((tp // 2, nb)),
+            dma((max(tp // 2 - 1, 1), nb)),
             dma((tp, nb)),
             dma((tp // 2, nb)),
             dma((tp // 2, nb)),

time: 168 us -> 168 us (level)
  no operation moved by 1% of the time
where the time goes in v5:
time: 168 us
  Pallas kernels  166 us (99%)
  local copies, waits for them, and re-layouts  2.26 us (1%)
    pallas_call x1, Pallas kernels, layer(): pl.pallas_call(functools.partial(layer_kernel, n, tp, heads, s1, s2, spli...  166 us

profile of v5, /device:TPU:28, one launch (start us, length us, event | category | flops | bytes accessed | tf_op | source)
XLA Modules:
  0.0 168.0 jit_solution(3958165925114994273)
XLA Ops:
  0.0 165.8 %layer.1 = bf16[1024,512]{1,0:T(8,128)(2,1)} custom-call(bf16[1024,2,256]{2,1,0:T(2,128)(2,1)} %x_ref.1, bf16[1024,128]{1,0:T(8,128)(2,1)} %keys1_ref.1, bf16[1024,128]{1,0:T(8,128)(2,1)} %queries1_ref.1, bf16[64,1024]{1,0:T(8,128)(2,1)} %bitcast.5, bf16[64,1024]{1,0:T(8,128)(2,1)} %bitcast.6, f32[2,4,1024]{2,1,0:T(4,128)} %bitcast.7, ...), custom_call_target="tpu_custom_call" | custom-call | tf_op jit(solution)/shard_map/layer/pallas_call | solution.py:970
  165.8 2.3 %copy.21 = bf16[1024,512]{1,0:T(8,128)(2,1)} copy(bf16[1024,512]{1,0:T(8,128)(2,1)} %layer.1) | data formatting | bytes 2097152
